TPU v7x, 32 devices: a whole 2x2x4 slice. The times are simulated.
32 devices in a mesh: ep: 4 (over y, x), tp: 8 (over z, core).
Axes of the slice: x: 2, y: 2, z: 4, core: 2. Of those that a mesh axis runs over, the one named last changes fastest.
Arguments:
- tokens: bfloat16 [128, 2048], P(('ep', 'tp')), may hold values from -6 to 6
- lengths: int32 [128], P(('ep', 'tp')), may hold values from 64 to 1024
- cache_latent: bfloat16 [128, 1024, 512], P(('ep', 'tp')), may hold values from -6 to 6
- cache_rope_key: bfloat16 [128, 1024, 32], P(('ep', 'tp')), may hold values from -1000 to 1000
- route_ids: int32 [128, 4], P('ep'), may hold values from 0 to 31, all different within a row; in each aligned block of 32 rows (0 to 31, 32 to 63, ...) at most 8 rows name the same one
- route_weights: float32 [128, 4], P('ep'), may hold values from 0.2 to 2
- attn_gain: float32 [2048], replicated, may hold values from 0.1 to 1.9
- w_query_nope: bfloat16 [2048, 16, 64], P(None, 'tp'), may hold values from -0.125 to 0.125
- w_query_rope: bfloat16 [2048, 16, 32], P(None, 'tp'), may hold values from -0.125 to 0.125
- w_latent_down: bfloat16 [2048, 512], P(None, 'tp'), may hold values from -0.125 to 0.125
- w_key_rope: bfloat16 [2048, 32], replicated, may hold values from -0.125 to 0.125
- latent_gain: float32 [512], replicated, may hold values from 0.1 to 1.9
- w_key_up: bfloat16 [512, 16, 64], P(None, 'tp'), may hold values from -0.75 to 0.75
- w_value_up: bfloat16 [512, 16, 64], P(None, 'tp'), may hold values from -0.25 to 0.25
- w_attn_out: bfloat16 [16, 64, 2048], P('tp'), may hold values from -0.1875 to 0.1875
- ffn_gain: float32 [2048], replicated, may hold values from 0.1 to 1.9
- expert_gate: bfloat16 [32, 2048, 512], P(('ep', 'tp')), may hold values from -0.125 to 0.125
- expert_up: bfloat16 [32, 2048, 512], P(('ep', 'tp')), may hold values from -0.125 to 0.125
- expert_down: bfloat16 [32, 512, 2048], P(('ep', 'tp')), may hold values from -0.25 to 0.25
- shared_gate: bfloat16 [2048, 512], P(None, 'tp'), may hold values from -0.125 to 0.125
- shared_up: bfloat16 [2048, 512], P(None, 'tp'), may hold values from -0.125 to 0.125
- shared_down: bfloat16 [512, 2048], P('tp'), may hold values from -0.25 to 0.25
- dense_gate: bfloat16 [2048, 1024], P(None, 'tp'), may hold values from -0.125 to 0.125
- dense_up: bfloat16 [2048, 1024], P(None, 'tp'), may hold values from -0.125 to 0.125
- dense_down: bfloat16 [1024, 2048], P('tp'), may hold values from -0.1875 to 0.1875
- branch_gate: bfloat16 [2048], replicated, may hold values from -0.125 to 0.125
Outputs:
- mixed: bfloat16 [128, 2048], P(('ep', 'tp'))
- new_latent: bfloat16 [128, 512], P(('ep', 'tp'))
- new_rope_key: bfloat16 [128, 32], P(('ep', 'tp'))
Inputs may be any that keep to these rules, and one draw needn't show every extreme that they name: `route_ids`: in each aligned block of 32 rows, no expert is named by more than 8 of the block's rows, a bound that some block reaches. Each row names 4 different experts.
All inputs are finite; a program needn't handle non-finite values.
Results may differ from a plain program's by a relative error of at most 0.025.
Values may be sent and summed in bfloat16 or wider, within the bound.
A program may use at most 64 MiB of HBM per device.

v0:
```python
import functools

import jax
import jax.numpy as jnp
import numpy as np
from jax import lax
from jax.experimental import pallas as pl
from jax.experimental.pallas import tpu as pltpu
from jax.sharding import PartitionSpec as P

epsilon = 1e-06
rope_base = 10000.0
lanes = 128
F32 = jnp.float32
BF16 = jnp.bfloat16
MESH = pl.DeviceIdType.MESH


def nn(a, b):
    return lax.dot_general(a, b, (((1,), (0,)), ((), ())), preferred_element_type=F32)


def nt(a, b):
    return lax.dot_general(a, b, (((1,), (1,)), ((), ())), preferred_element_type=F32)


def tn(a, b):
    return lax.dot_general(a, b, (((0,), (0,)), ((), ())), preferred_element_type=F32)


def join(pieces):
    return pieces[0] if len(pieces) == 1 else jnp.concatenate(pieces, axis=0)


def flipped(index, mask, count):
    out = index
    bit = 1
    while bit < count:
        if mask & bit:
            out = out + bit - 2 * bit * (index // bit % 2)
        bit *= 2
    return out


def flat(ref):
    return jnp.concatenate([ref[i : i + 1, :] for i in range(ref.shape[0])], axis=1)


def spread(values, count):
    rows = values.shape[0]
    return join(
        [jnp.broadcast_to(values[b : b + 1], (count, values.shape[1])) for b in range(rows)]
    )


def rows_of(ref, count):
    return join([ref[i].astype(F32) for i in range(count)])


def factor_of(values):
    return lax.rsqrt(jnp.mean(values * values, axis=-1, keepdims=True) + epsilon)


def silu(v):
    return v / (1.0 + jnp.exp(-v))


def lane_block(values, column, width):
    base, offset = column // lanes * lanes, column % lanes
    block = values[:, base : base + lanes]
    if offset:
        block = pltpu.roll(block, lanes - offset, 1)
    lane = lax.broadcasted_iota(jnp.int32, block.shape, 1)
    return jnp.where(lane < width, block, 0.0)


def turn(values, cosine, sine, half):
    lane = lax.broadcasted_iota(jnp.int32, values.shape, 1)
    swapped = jnp.where(
        lane < half, -pltpu.roll(values, lanes - half, 1), pltpu.roll(values, half, 1)
    )
    return values * cosine + swapped * sine


def layer(
    sizes,
    turns, tokens, ids, wts, attn_gain, ffn_gain, latent_gain, branch_gate, lengths,
    wqn, wqr, wld, wkr, cl, cr, wku, wvu, wo, sg, su, dg, du, sd, dd, eg, eu, ed,
    mixed, newlat, newrope,
    v_in, v_kr, v_cl, v_cr, v_ku, v_vu, v_wo, v_sg, v_su, v_dg, v_du, v_sd, v_dd, v_eg, v_eu, v_ed,
    agx, sendq, recvq, sendo, recvo, senda, recva, agf, sende, recve, sendr, recvr, sendf, recvf,
    half_a, whole_a,
    kr_pad, w_sem, tp_send, tp_recv, ep_send, ep_recv,
):
    T, EP, own, H, nope, rope, latent, cap, scale = sizes
    group = T * own
    R = H * own
    me_t = lax.axis_index("tp")
    me_e = lax.axis_index("ep")
    lat_w = wld.shape[0]

    barrier = pltpu.get_barrier_semaphore()
    for k in range(1, T):
        pl.semaphore_signal(
            barrier, inc=1, device_id=(me_e, flipped(me_t, k, T)), device_id_type=MESH
        )
    for k in range(1, EP):
        pl.semaphore_signal(
            barrier, inc=1, device_id=(flipped(me_e, k, EP), me_t), device_id_type=MESH
        )

    n_q, n_r = H * nope, H * rope
    pairs = [
        (wqn, v_in.at[pl.ds(0, n_q)]),
        (wqr, v_in.at[pl.ds(n_q, n_r)]),
        (wld, v_in.at[pl.ds(n_q + n_r, lat_w)]),
        (wkr, v_kr),
        (wku, v_ku),
    ]
    first_cl = len(pairs)
    pairs += [(cl.at[b], v_cl.at[b]) for b in range(own)]
    first_rest = len(pairs)
    pairs += [(cr, v_cr), (wvu, v_vu), (wo, v_wo)]
    first_ffn = len(pairs)
    pairs += [
        (sg, v_sg), (su, v_su), (dg, v_dg), (du, v_du), (sd, v_sd), (dd, v_dd),
        (eg, v_eg), (eu, v_eu), (ed, v_ed),
    ]
    loads = [
        pltpu.make_async_copy(src, dst, w_sem.at[i]) for i, (src, dst) in enumerate(pairs)
    ]
    for load in loads:
        load.start()

    sends = []

    def tp_exchange(phase, source, target):
        out = []
        for k in range(T - 1, 0, -1):
            peer = flipped(me_t, k, T)
            out.append(
                pltpu.make_async_remote_copy(
                    src_ref=source(peer),
                    dst_ref=target.at[me_t],
                    send_sem=tp_send.at[phase, k],
                    recv_sem=tp_recv.at[phase, k],
                    device_id=(me_e, peer),
                    device_id_type=MESH,
                )
            )
        for c in out:
            c.start()
        sends.extend(out)
        return out

    def tp_copy(phase, k, source, target, peer):
        c = pltpu.make_async_remote_copy(
            src_ref=source,
            dst_ref=target,
            send_sem=tp_send.at[phase, k],
            recv_sem=tp_recv.at[phase, k],
            device_id=(me_e, peer),
            device_id_type=MESH,
        )
        c.start()
        sends.append(c)
        return c

    partner = flipped(me_t, 1, T)
    across = list(range(T - 2, 0, -2))

    def tp_gather(phase, target):
        mine = target.at[me_t]
        direct = [(m, tp_copy(phase, m, mine, mine, flipped(me_t, m, T))) for m in across]
        out = [tp_copy(phase, 1, mine, mine, partner)]

        def finish():
            for m, c in reversed(direct):
                c.wait_recv()
                block = target.at[flipped(me_t, m, T)]
                out.append(tp_copy(phase, m + 1, block, block, partner))
            for c in out:
                c.wait_recv()

        return finish

    def tp_scatter(phase, source, half, whole, target):
        first = []
        for m in across + [0]:
            to = flipped(partner, m, T)
            first.append((m, tp_copy(phase, m + 1, source.at[to], half.at[to], partner)))
        out = []
        for m, c in first:
            c.wait_recv()
            to = flipped(me_t, m, T)
            both = (source[to].astype(F32) + half[to].astype(F32)).astype(BF16)
            if m == 0:
                target[me_t] = both
            else:
                whole[to] = both
                out.append(tp_copy(phase, m, whole.at[to], target.at[me_t], to))
        for c in out:
            c.wait_recv()
        total = target[me_t].astype(F32)
        for m in across:
            total = total + target[flipped(me_t, m, T)].astype(F32)
        return total

    def ep_exchange(phase, source, target):
        out = []
        for k in range(EP - 1, 0, -1):
            peer = flipped(me_e, k, EP)
            out.append(
                pltpu.make_async_remote_copy(
                    src_ref=source.at[peer],
                    dst_ref=target.at[me_e],
                    send_sem=ep_send.at[phase, k],
                    recv_sem=ep_recv.at[phase, k],
                    device_id=(peer, me_t),
                    device_id_type=MESH,
                )
            )
        for c in out:
            c.start()
        sends.extend(out)
        return out

    def arrive(copies):
        for c in copies:
            c.wait_recv()

    x = tokens[...].astype(F32)
    normed = (x * factor_of(x) * flat(attn_gain[...])).astype(BF16)
    agx[me_t] = normed
    pl.semaphore_wait(barrier, T - 1 + EP - 1)
    finish = tp_gather(0, agx)

    slots = EP * cap
    slot = lax.broadcasted_iota(jnp.int32, (slots, group), 0)
    block = jnp.zeros((slots, group), jnp.int32)
    for j in range(1, EP):
        block = block + jnp.where(slot >= j * cap, 1, 0)
    expert = block * T + me_t
    place = (slot - block * cap).astype(F32)
    hit = jnp.zeros((slots, group), F32)
    weight = jnp.zeros((slots, group), F32)
    for k in range(ids.shape[0]):
        same = ids[k : k + 1, :] == expert
        hit = hit + jnp.where(same, 1.0, 0.0)
        weight = weight + jnp.where(same, wts[k : k + 1, :], 0.0)
    upper = jnp.where(
        lax.broadcasted_iota(jnp.int32, (group, group), 0)
        < lax.broadcasted_iota(jnp.int32, (group, group), 1),
        1.0,
        0.0,
    ).astype(BF16)
    rank = nn(hit.astype(BF16), upper)
    dispatch = jnp.where(rank == place, hit, 0.0)
    weight = weight * dispatch
    weight_hi = weight.astype(BF16)
    weight_lo = (weight - weight_hi.astype(F32)).astype(BF16)
    dispatch = dispatch.astype(BF16)

    for i in range(first_cl):
        loads[i].wait()
    left = jnp.zeros((own, lanes), jnp.int32)
    row = lax.broadcasted_iota(jnp.int32, (own, lanes), 0)
    for b in range(own):
        left = jnp.where(row == b, lengths[b], left)
    length = left
    bits = turns.shape[0] // 2
    cosine = jnp.ones((own, lanes), F32)
    sine = jnp.zeros((own, lanes), F32)
    for i in range(bits - 1, -1, -1):
        has = left >= 2**i
        left = jnp.where(has, left - 2**i, left)
        c, s = turns[i : i + 1, :], turns[bits + i : bits + i + 1, :]
        cosine, sine = (
            jnp.where(has, cosine * c - sine * s, cosine),
            jnp.where(has, cosine * s + sine * c, sine),
        )
    live = lax.broadcasted_iota(jnp.int32, (own, lanes), 1) < rope
    cosine = jnp.where(live, cosine, 0.0)
    sine = jnp.where(live, sine, 0.0)
    big = T * H
    at = lax.broadcasted_iota(jnp.int32, (own * big, own * big), 0)
    to = lax.broadcasted_iota(jnp.int32, (own * big, own * big), 1)

    def from_row(r):
        seq = jnp.zeros_like(r)
        for i in range(1, own):
            seq = seq + jnp.where(r >= i * big, 1, 0)
        return (r - seq * big) * own + seq

    to_seq = jnp.where(to == from_row(at), 1.0, 0.0).astype(BF16)
    to_dev = jnp.where(at == from_row(to), 1.0, 0.0).astype(BF16)
    kr_pad[...] = jnp.zeros_like(kr_pad)
    kr_pad[:, 0:rope] = nt(normed, v_kr[...])
    new_rope = turn(kr_pad[...], cosine, sine, rope // 2).astype(BF16)
    newrope[...] = new_rope[:, 0:rope]

    finish()
    rows = rows_of(agx, T).astype(BF16)
    proj = nt(rows, v_in[...])
    q_lat = [
        nn(lane_block(proj, h * nope, nope)[:, 0:nope].astype(BF16), v_ku[h]) for h in range(H)
    ]
    q_rope = [lane_block(proj, n_q + h * rope, rope) for h in range(H)]
    lat_part = pltpu.roll(lane_block(proj, n_q + n_r, lat_w), lanes - lat_w, 1)
    for u in range(T):
        cut = slice(own * u, own * (u + 1))
        sendq[u, :, 0:latent] = join([q[cut] for q in q_lat]).astype(BF16)
        sendq[u, :, latent : latent + lanes] = join(
            [q[cut] + lat_part[cut] for q in q_rope]
        ).astype(BF16)
    step = tp_exchange(1, lambda peer: sendq.at[peer], recvq)
    recvq[me_t] = sendq[me_t]
    for i in range(first_cl, first_ffn):
        loads[i].wait()
    arrive(step)

    queries = rows_of(recvq, T)
    per = lanes // lat_w
    lane = lax.broadcasted_iota(jnp.int32, (own, lanes), 1)
    blocks = []
    for j in range(T // per):
        total = None
        for i in range(per):
            top = R * (j * per + i)
            piece = jnp.where(lane >= lanes - lat_w, queries[top : top + own, latent:], 0.0)
            if i < per - 1:
                piece = pltpu.roll(piece, (i + 1) * lat_w, 1)
            total = piece if total is None else total + piece
        blocks.append(total)
    raw = blocks[0] if len(blocks) == 1 else jnp.concatenate(blocks, axis=1)
    new_latent = (raw * factor_of(raw) * flat(latent_gain[...])).astype(BF16)
    newlat[...] = new_latent
    new_lat32, new_rope32 = new_latent.astype(F32), new_rope.astype(F32)
    queries = nn(to_seq, queries.astype(BF16))
    q_rot = turn(
        jnp.where(
            lax.broadcasted_iota(jnp.int32, (own * big, lanes), 1) < rope, queries[:, latent:], 0.0
        ),
        spread(cosine, big),
        spread(sine, big),
        rope // 2,
    ).astype(BF16)
    q_lat32 = queries[:, 0:latent]
    outs = []
    for b in range(own):
        cut = slice(big * b, big * (b + 1))
        q_b, r_b = q_lat32[cut], q_rot.astype(F32)[cut]
        lat_b, rope_b = new_lat32[b : b + 1], new_rope32[b : b + 1]
        own_score = (
            jnp.sum(q_b * lat_b, axis=-1, keepdims=True)
            + jnp.sum(r_b * rope_b, axis=-1, keepdims=True)
        ) * scale
        scores = nt(q_b.astype(BF16), v_cl[b]) + nn(r_b[:, 0:rope].astype(BF16), v_cr[b])
        position = lax.broadcasted_iota(jnp.int32, scores.shape, 1)
        scores = jnp.where(position < length[b : b + 1, 0:1], scores * scale, -jnp.inf)
        peak = jnp.maximum(jnp.max(scores, axis=-1, keepdims=True), own_score)
        past = jnp.exp(scores - peak)
        own_exp = jnp.exp(own_score - peak)
        total = jnp.sum(past, axis=-1, keepdims=True) + own_exp
        past = (past / total).astype(BF16)
        own_weight = (own_exp / total).astype(BF16).astype(F32)
        outs.append(nn(past, v_cl[b]) + own_weight * lat_b)
    mixed_lat = nn(to_dev, join(outs).astype(BF16))
    for u in range(T):
        sendo[u] = mixed_lat[R * u : R * (u + 1)].astype(BF16)
    step = tp_exchange(2, lambda peer: sendo.at[peer], recvo)
    recvo[me_t] = sendo[me_t]
    arrive(step)

    back = rows_of(recvo, T).astype(BF16)
    part = None
    for h in range(H):
        values = nt(back, v_vu[h])
        values = join(
            [values[R * u + own * h : R * u + own * (h + 1)] for u in range(T)]
        ).astype(BF16)
        term = nn(values, v_wo[h])
        part = term if part is None else part + term
    for u in range(T):
        senda[u] = part[own * u : own * (u + 1)].astype(BF16)
    after = tokens[...].astype(F32) + tp_scatter(3, senda, half_a, whole_a, recva)
    agf[me_t] = (after * factor_of(after) * flat(ffn_gain[...])).astype(BF16)
    finish = tp_gather(4, agf)
    for i in range(first_ffn, len(loads)):
        loads[i].wait()
    finish()

    rows32 = rows_of(agf, T)
    rows = rows32.astype(BF16)
    outgoing = nn(dispatch, rows)
    for j in range(EP):
        sende[j] = outgoing[cap * j : cap * (j + 1)].astype(BF16)
    step = ep_exchange(0, sende, recve)
    recve[me_e] = sende[me_e]

    act = (silu(nt(rows, v_sg[...])) * nt(rows, v_su[...])).astype(BF16)
    ffn = nn(act, v_sd[...])
    gate = jnp.sum(rows32 * flat(branch_gate[...].astype(F32)), axis=-1, keepdims=True)
    gate = 1.0 / (1.0 + jnp.exp(-gate))
    act = (silu(nn(rows, v_dg[...])) * nn(rows, v_du[...])).astype(BF16)
    ffn = ffn + gate * nn(act, v_dd[...])

    arrive(step)
    routed = rows_of(recve, EP).astype(BF16)
    act = (silu(nn(routed, v_eg[...])) * nn(routed, v_eu[...])).astype(BF16)
    wide = v_ed.shape[1] // 2
    cuts = [slice(0, wide), slice(wide, 2 * wide)]
    steps = []
    for n, cut in enumerate(cuts):
        result = nn(act, v_ed[:, cut])
        for j in range(EP):
            sendr[n, j] = result[cap * j : cap * (j + 1)].astype(BF16)
        steps.append(ep_exchange(1 + n, sendr.at[n], recvr.at[n]))
        recvr[n, me_e] = sendr[n, me_e]
    last = []
    for n, cut in enumerate(cuts):
        arrive(steps[n])
        returned = rows_of(recvr.at[n], EP).astype(BF16)
        part = ffn[:, cut] + (tn(weight_hi, returned) + tn(weight_lo, returned))
        for u in range(T):
            sendf[n, u] = part[own * u : own * (u + 1)].astype(BF16)
        last.append(tp_exchange(5 + n, lambda peer: sendf.at[n, peer], recvf.at[n]))
        recvf[n, me_t] = sendf[n, me_t]
    for n, cut in enumerate(cuts):
        arrive(last[n])
        part = after[:, cut]
        for u in range(T):
            part = part + recvf[n, u].astype(F32)
        mixed[:, cut] = part.astype(BF16)
    for c in sends:
        c.wait_send()


def hand_over(*refs):
    half = len(refs) // 2
    for source, target in zip(refs[:half], refs[half:]):
        target[...] = source[...]


def local(
    tokens, lengths, cache_latent, cache_rope_key, route_ids, route_weights, attn_gain,
    w_query_nope, w_query_rope, w_latent_down, w_key_rope, latent_gain, w_key_up, w_value_up,
    w_attn_out, ffn_gain, expert_gate, expert_up, expert_down, shared_gate, shared_up,
    shared_down, dense_gate, dense_up, dense_down, branch_gate,
):
    own, width = tokens.shape
    T = lax.axis_size("tp")
    EP = lax.axis_size("ep")
    H, nope = w_query_nope.shape[1:]
    rope = w_query_rope.shape[2]
    latent = cache_latent.shape[2]
    top = route_ids.shape[1]
    assert expert_gate.shape[0] == 1
    cap = max(2, (2 * own * top + EP - 1) // EP)
    R = H * own
    half = rope // 2

    bits = cache_latent.shape[1].bit_length()
    frequencies = (rope_base ** (-np.arange(half) / half)).astype(np.float32).astype(np.float64)
    angles = frequencies[None, :] * 2.0 ** np.arange(bits)[:, None]
    angles = np.pad(np.tile(angles, (1, 2)), ((0, 0), (0, lanes - rope)))
    turns = jnp.asarray(np.concatenate([np.cos(angles), np.sin(angles)]), F32)

    operands = (
        turns,
        tokens,
        route_ids.T,
        route_weights.T,
        attn_gain.reshape(-1, lanes),
        ffn_gain.reshape(-1, lanes),
        latent_gain.reshape(-1, lanes),
        branch_gate.reshape(-1, lanes),
        lengths,
        w_query_nope.transpose(1, 2, 0).reshape(H * nope, width),
        w_query_rope.transpose(1, 2, 0).reshape(H * rope, width),
        w_latent_down.T,
        w_key_rope.T,
        cache_latent,
        cache_rope_key.transpose(0, 2, 1),
        w_key_up.transpose(1, 2, 0),
        w_value_up.transpose(1, 2, 0),
        w_attn_out,
        shared_gate.T,
        shared_up.T,
        dense_gate,
        dense_up,
        shared_down,
        dense_down,
        expert_gate[0],
        expert_up[0],
        expert_down[0],
    )
    big = operands[9:]
    v_in = pltpu.VMEM((sum(o.shape[0] for o in big[:3]), width), BF16)
    weights = [v_in] + [pltpu.VMEM(o.shape, BF16) for o in big[3:]]
    q_width = latent + lanes

    def comm(*shape):
        return pltpu.VMEM(shape, BF16)

    buffers = [
        comm(T, own, width),
        comm(T, R, q_width), comm(T, R, q_width),
        comm(T, R, latent), comm(T, R, latent),
        comm(T, own, width), comm(T, own, width),
        comm(T, own, width),
        comm(EP, cap, width), comm(EP, cap, width),
        comm(2, EP, cap, width // 2), comm(2, EP, cap, width // 2),
        comm(2, T, own, width // 2), comm(2, T, own, width // 2),
        comm(T, own, width), comm(T, own, width),
        pltpu.VMEM((own, lanes), F32),
    ]
    n_loads = len(big) + own - 1
    sems = [
        pltpu.SemaphoreType.DMA((n_loads,)),
        pltpu.SemaphoreType.DMA((7, T)),
        pltpu.SemaphoreType.DMA((7, T)),
        pltpu.SemaphoreType.DMA((3, EP)),
        pltpu.SemaphoreType.DMA((3, EP)),
    ]
    sizes = (T, EP, own, H, nope, rope, latent, cap, (nope + rope) ** (-0.5))
    vmem = pl.BlockSpec(memory_space=pltpu.VMEM)
    results = pl.pallas_call(
        functools.partial(layer, sizes),
        out_shape=(
            jax.ShapeDtypeStruct((own, width), BF16),
            jax.ShapeDtypeStruct((own, latent), BF16),
            jax.ShapeDtypeStruct((own, rope), BF16),
        ),
        in_specs=[vmem] * 8
        + [pl.BlockSpec(memory_space=pltpu.SMEM)]
        + [pl.BlockSpec(memory_space=pl.ANY)] * len(big),
        out_specs=(vmem, vmem, vmem),
        scratch_shapes=weights + buffers + sems,
        compiler_params=pltpu.CompilerParams(collective_id=0, has_side_effects=True),
    )(*operands)
    return pl.pallas_call(
        hand_over,
        out_shape=tuple(jax.ShapeDtypeStruct(r.shape, r.dtype) for r in results),
        in_specs=[vmem] * 3,
        out_specs=(vmem, vmem, vmem),
    )(*results)


def solution(mesh):
    both = ("ep", "tp")
    in_specs = (
        P(both, None),
        P(both),
        P(both, None, None),
        P(both, None, None),
        P("ep", None),
        P("ep", None),
        P(),
        P(None, "tp", None),
        P(None, "tp", None),
        P(None, "tp"),
        P(),
        P(),
        P(None, "tp", None),
        P(None, "tp", None),
        P("tp", None, None),
        P(),
        P(both, None, None),
        P(both, None, None),
        P(both, None, None),
        P(None, "tp"),
        P(None, "tp"),
        P("tp", None),
        P(None, "tp"),
        P(None, "tp"),
        P("tp", None),
        P(),
    )
    out_specs = (P(both, None), P(both, None), P(both, None))
    return jax.shard_map(local, mesh=mesh, in_specs=in_specs, out_specs=out_specs, check_vma=False)
```

profile of v0, /device:TPU:0, one launch (start us, length us, event | category | flops | bytes accessed | tf_op | source)
XLA Modules:
  0.0 48.9 jit_solution(13548703662087857609)
XLA Ops:
  0.6 47.0 %shard_map.274 = (bf16[4,2048]{1,0:T(4,128)(2,1)}, bf16[4,512]{1,0:T(4,128)(2,1)}, bf16[4,32]{1,0:T(4,128)(2,1)}) custom-call(f32[22,128]{1,0:T(8,128)} %constant.2.clone.turns, bf16[4,2048]{1,0:T(4,128)(2,1)} %tokens.1, s32[4,32]{1,0:T(4,128)} %bitcast.37, f32[4,32]{1,0:T(4,128)} %bitcast.38, f32[16,128]{1,0:T(8,128)} %bitcast.34, f32[16,128]{1,0:T(8,128)} %bitcast.35, ...), custom_call_target="tpu_custom_call" | custom-call | tf_op jit(solution)/shard_map/pallas_call | solution.py:528
  47.6 1.3 %shard_map.275 = (bf16[4,2048]{1,0:T(4,128)(2,1)}, bf16[4,512]{1,0:T(4,128)(2,1)}, bf16[4,32]{1,0:T(4,128)(2,1)}) custom-call(bf16[4,2048]{1,0:T(4,128)(2,1)} %get-tuple-element.6.refs_0_, bf16[4,512]{1,0:T(4,128)(2,1)} %get-tuple-element.7.refs_1_, bf16[4,32]{1,0:T(4,128)(2,1)} %get-tuple-element.8.refs_2_), custom_call_target="tpu_custom_call" | custom-call | tf_op jit(solution)/shard_map/pallas_call | solution.py:542
where the time goes:
time: 49.2 us; the launch traced here: 48.9 us
  Pallas kernels  48.3 us (98%)
  between operations  0.65 us (1%)
    pallas_call x1, Pallas kernels, local(): pl.pallas_call(functools.partial(layer, sizes), out_shape=(jax.ShapeDtype...  47 us
    pallas_call x1, Pallas kernels, local(): pl.pallas_call(hand_over, out_shape=tuple((jax.ShapeDtypeStruct(r.shape,...  1.34 us

commit v1 on v0

--- a/solution.py
+++ b/solution.py
@@ -42,6 +42,22 @@
     return out
 
 
+def far_first(me, chips, cores):
+    chip, core = me // cores, me % cores
+    low = 1 - chip // (chips // 2)
+    order = []
+    for i in range(chips - 1):
+        down = chips - 1 - i
+        down = down - (chip - down + chips) // chips
+        up = i + (i - chip + chips) // chips
+        to = low * down + (1 - low) * up
+        for turn_core in range(cores):
+            order.append(to * cores + (core + turn_core) % cores)
+    for turn_core in range(1, cores):
+        order.append(chip * cores + (core + turn_core) % cores)
+    return order
+
+
 def flat(ref):
     return jnp.concatenate([ref[i : i + 1, :] for i in range(ref.shape[0])], axis=1)
 
@@ -84,12 +100,12 @@
 
 def layer(
     sizes,
-    turns, tokens, ids, wts, attn_gain, ffn_gain, latent_gain, branch_gate, lengths,
+    h_tokens, h_attn_gain, h_lengths, h_turns, h_ids, h_wts, h_ffn_gain, h_latent_gain, h_branch_gate,
     wqn, wqr, wld, wkr, cl, cr, wku, wvu, wo, sg, su, dg, du, sd, dd, eg, eu, ed,
     mixed, newlat, newrope,
-    v_in, v_kr, v_cl, v_cr, v_ku, v_vu, v_wo, v_sg, v_su, v_dg, v_du, v_sd, v_dd, v_eg, v_eu, v_ed,
+    tokens, attn_gain, lengths, turns, ids, wts, ffn_gain, latent_gain, branch_gate,
+    v_in, v_kr, v_cl, v_cr, v_ku, v_vu, v_wo, v_s, v_d, v_sd, v_dd, v_e, v_ed,
     agx, sendq, recvq, sendo, recvo, senda, recva, agf, sende, recve, sendr, recvr, sendf, recvf,
-    half_a, whole_a,
     kr_pad, w_sem, tp_send, tp_recv, ep_send, ep_recv,
 ):
     T, EP, own, H, nope, rope, latent, cap, scale = sizes
@@ -110,130 +126,106 @@
         )
 
     n_q, n_r = H * nope, H * rope
-    pairs = [
-        (wqn, v_in.at[pl.ds(0, n_q)]),
-        (wqr, v_in.at[pl.ds(n_q, n_r)]),
-        (wld, v_in.at[pl.ds(n_q + n_r, lat_w)]),
-        (wkr, v_kr),
-        (wku, v_ku),
+    groups = [
+        [(h_tokens, tokens)],
+        [(h_attn_gain, attn_gain)],
+        [
+            (wqn, v_in.at[pl.ds(0, n_q)]),
+            (wqr, v_in.at[pl.ds(n_q, n_r)]),
+            (wld, v_in.at[pl.ds(n_q + n_r, lat_w)]),
+        ],
+        [(wkr, v_kr)],
+        [(wku, v_ku)],
+        [(h_lengths, lengths)],
+        [(h_turns, turns)],
+        [(h_ids, ids)],
+        [(h_wts, wts)],
+        [(cl, v_cl)],
+        [(cr, v_cr)],
+        [(wvu, v_vu)],
+        [(wo, v_wo)],
+        [(h_latent_gain, latent_gain)],
+        [(h_ffn_gain, ffn_gain)],
+        [(sg, v_s.at[0]), (su, v_s.at[1])],
+        [(dg, v_d.at[0]), (du, v_d.at[1])],
+        [(sd, v_sd)],
+        [(dd, v_dd)],
+        [(h_branch_gate, branch_gate)],
+        [(eg, v_e.at[0]), (eu, v_e.at[1])],
+        [(ed, v_ed)],
     ]
-    first_cl = len(pairs)
-    pairs += [(cl.at[b], v_cl.at[b]) for b in range(own)]
-    first_rest = len(pairs)
-    pairs += [(cr, v_cr), (wvu, v_vu), (wo, v_wo)]
-    first_ffn = len(pairs)
-    pairs += [
-        (sg, v_sg), (su, v_su), (dg, v_dg), (du, v_du), (sd, v_sd), (dd, v_dd),
-        (eg, v_eg), (eu, v_eu), (ed, v_ed),
-    ]
-    loads = [
-        pltpu.make_async_copy(src, dst, w_sem.at[i]) for i, (src, dst) in enumerate(pairs)
-    ]
-    for load in loads:
-        load.start()
+    wholes = {2: v_in, 15: v_s, 16: v_d, 20: v_e}
+    first_small, first_cl, first_ffn = 2, 9, 15
+    loads = []
+    for i, bunch in enumerate(groups):
+        for source, target in bunch:
+            load = pltpu.make_async_copy(source, target, w_sem.at[i])
+            load.start()
+        if len(bunch) > 1:
+            load = pltpu.make_async_copy(wholes[i], wholes[i], w_sem.at[i])
+        loads.append(load)
 
     sends = []
 
+    order = far_first(me_t, T // 2, 2)
+
     def tp_exchange(phase, source, target):
-        out = []
-        for k in range(T - 1, 0, -1):
-            peer = flipped(me_t, k, T)
-            out.append(
-                pltpu.make_async_remote_copy(
-                    src_ref=source(peer),
-                    dst_ref=target.at[me_t],
-                    send_sem=tp_send.at[phase, k],
-                    recv_sem=tp_recv.at[phase, k],
-                    device_id=(me_e, peer),
-                    device_id_type=MESH,
-                )
-            )
-        for c in out:
-            c.start()
-        sends.extend(out)
-        return out
-
-    def tp_copy(phase, k, source, target, peer):
-        c = pltpu.make_async_remote_copy(
-            src_ref=source,
-            dst_ref=target,
-            send_sem=tp_send.at[phase, k],
-            recv_sem=tp_recv.at[phase, k],
-            device_id=(me_e, peer),
+        for peer in order:
+            pltpu.make_async_remote_copy(
+                src_ref=source(peer),
+                dst_ref=target.at[me_t],
+                send_sem=tp_send.at[phase],
+                recv_sem=tp_recv.at[phase],
+                device_id=(me_e, peer),
+                device_id_type=MESH,
+            ).start()
+        blocks = target.at[pl.ds(0, T - 1)]
+        every = pltpu.make_async_remote_copy(
+            src_ref=blocks,
+            dst_ref=blocks,
+            send_sem=tp_send.at[phase],
+            recv_sem=tp_recv.at[phase],
+            device_id=(me_e, order[0]),
             device_id_type=MESH,
         )
-        c.start()
-        sends.append(c)
-        return c
-
-    partner = flipped(me_t, 1, T)
-    across = list(range(T - 2, 0, -2))
-
-    def tp_gather(phase, target):
-        mine = target.at[me_t]
-        direct = [(m, tp_copy(phase, m, mine, mine, flipped(me_t, m, T))) for m in across]
-        out = [tp_copy(phase, 1, mine, mine, partner)]
-
-        def finish():
-            for m, c in reversed(direct):
-                c.wait_recv()
-                block = target.at[flipped(me_t, m, T)]
-                out.append(tp_copy(phase, m + 1, block, block, partner))
-            for c in out:
-                c.wait_recv()
-
-        return finish
-
-    def tp_scatter(phase, source, half, whole, target):
-        first = []
-        for m in across + [0]:
-            to = flipped(partner, m, T)
-            first.append((m, tp_copy(phase, m + 1, source.at[to], half.at[to], partner)))
-        out = []
-        for m, c in first:
-            c.wait_recv()
-            to = flipped(me_t, m, T)
-            both = (source[to].astype(F32) + half[to].astype(F32)).astype(BF16)
-            if m == 0:
-                target[me_t] = both
-            else:
-                whole[to] = both
-                out.append(tp_copy(phase, m, whole.at[to], target.at[me_t], to))
-        for c in out:
-            c.wait_recv()
-        total = target[me_t].astype(F32)
-        for m in across:
-            total = total + target[flipped(me_t, m, T)].astype(F32)
-        return total
+        sends.append(every)
+        return every
 
     def ep_exchange(phase, source, target):
-        out = []
         for k in range(EP - 1, 0, -1):
             peer = flipped(me_e, k, EP)
-            out.append(
-                pltpu.make_async_remote_copy(
-                    src_ref=source.at[peer],
-                    dst_ref=target.at[me_e],
-                    send_sem=ep_send.at[phase, k],
-                    recv_sem=ep_recv.at[phase, k],
-                    device_id=(peer, me_t),
-                    device_id_type=MESH,
-                )
-            )
-        for c in out:
-            c.start()
-        sends.extend(out)
-        return out
-
-    def arrive(copies):
-        for c in copies:
-            c.wait_recv()
-
+            pltpu.make_async_remote_copy(
+                src_ref=source.at[peer],
+                dst_ref=target.at[me_e],
+                send_sem=ep_send.at[phase],
+                recv_sem=ep_recv.at[phase],
+                device_id=(peer, me_t),
+                device_id_type=MESH,
+            ).start()
+        blocks = target.at[pl.ds(0, EP - 1)]
+        every = pltpu.make_async_remote_copy(
+            src_ref=blocks,
+            dst_ref=blocks,
+            send_sem=ep_send.at[phase],
+            recv_sem=ep_recv.at[phase],
+            device_id=(flipped(me_e, 1, EP), me_t),
+            device_id_type=MESH,
+        )
+        sends.append(every)
+        return every
+
+    def arrive(step):
+        step.wait_recv()
+
+    for i in range(first_small):
+        loads[i].wait()
     x = tokens[...].astype(F32)
     normed = (x * factor_of(x) * flat(attn_gain[...])).astype(BF16)
     agx[me_t] = normed
     pl.semaphore_wait(barrier, T - 1 + EP - 1)
-    finish = tp_gather(0, agx)
+    step = tp_exchange(0, lambda peer: agx.at[me_t], agx)
+    for i in range(first_small, first_cl):
+        loads[i].wait()
 
     slots = EP * cap
     slot = lax.broadcasted_iota(jnp.int32, (slots, group), 0)
@@ -261,8 +253,6 @@
     weight_lo = (weight - weight_hi.astype(F32)).astype(BF16)
     dispatch = dispatch.astype(BF16)
 
-    for i in range(first_cl):
-        loads[i].wait()
     left = jnp.zeros((own, lanes), jnp.int32)
     row = lax.broadcasted_iota(jnp.int32, (own, lanes), 0)
     for b in range(own):
@@ -283,25 +273,25 @@
     cosine = jnp.where(live, cosine, 0.0)
     sine = jnp.where(live, sine, 0.0)
     big = T * H
-    at = lax.broadcasted_iota(jnp.int32, (own * big, own * big), 0)
-    to = lax.broadcasted_iota(jnp.int32, (own * big, own * big), 1)
-
-    def from_row(r):
-        seq = jnp.zeros_like(r)
-        for i in range(1, own):
-            seq = seq + jnp.where(r >= i * big, 1, 0)
-        return (r - seq * big) * own + seq
-
-    to_seq = jnp.where(to == from_row(at), 1.0, 0.0).astype(BF16)
-    to_dev = jnp.where(at == from_row(to), 1.0, 0.0).astype(BF16)
+    seq = lax.broadcasted_iota(jnp.int32, (own * big, lanes), 0) % own
+
+    def tiled(values):
+        return join([values] * big)
+
+    mine = [seq == b for b in range(own)]
+    length = tiled(length)
+    cosines, sines = tiled(cosine), tiled(sine)
     kr_pad[...] = jnp.zeros_like(kr_pad)
     kr_pad[:, 0:rope] = nt(normed, v_kr[...])
     new_rope = turn(kr_pad[...], cosine, sine, rope // 2).astype(BF16)
     newrope[...] = new_rope[:, 0:rope]
 
-    finish()
+    arrive(step)
     rows = rows_of(agx, T).astype(BF16)
-    proj = nt(rows, v_in[...])
+    wide = v_in.shape[0] // 2
+    proj = jnp.concatenate(
+        [nt(rows, v_in[0:wide, :]), nt(rows, v_in[wide : 2 * wide, :])], axis=1
+    )
     q_lat = [
         nn(lane_block(proj, h * nope, nope)[:, 0:nope].astype(BF16), v_ku[h]) for h in range(H)
     ]
@@ -336,36 +326,58 @@
     new_latent = (raw * factor_of(raw) * flat(latent_gain[...])).astype(BF16)
     newlat[...] = new_latent
     new_lat32, new_rope32 = new_latent.astype(F32), new_rope.astype(F32)
-    queries = nn(to_seq, queries.astype(BF16))
     q_rot = turn(
         jnp.where(
             lax.broadcasted_iota(jnp.int32, (own * big, lanes), 1) < rope, queries[:, latent:], 0.0
         ),
-        spread(cosine, big),
-        spread(sine, big),
+        cosines,
+        sines,
         rope // 2,
-    ).astype(BF16)
+    ).astype(BF16).astype(F32)
     q_lat32 = queries[:, 0:latent]
-    outs = []
+    new_lat_all = tiled(new_lat32)
+    own_score = (
+        jnp.sum(q_lat32 * new_lat_all, axis=-1, keepdims=True)
+        + jnp.sum(q_rot * tiled(new_rope32), axis=-1, keepdims=True)
+    ) * scale
+    across = None
+    wide_q = []
     for b in range(own):
-        cut = slice(big * b, big * (b + 1))
-        q_b, r_b = q_lat32[cut], q_rot.astype(F32)[cut]
-        lat_b, rope_b = new_lat32[b : b + 1], new_rope32[b : b + 1]
-        own_score = (
-            jnp.sum(q_b * lat_b, axis=-1, keepdims=True)
-            + jnp.sum(r_b * rope_b, axis=-1, keepdims=True)
-        ) * scale
-        scores = nt(q_b.astype(BF16), v_cl[b]) + nn(r_b[:, 0:rope].astype(BF16), v_cr[b])
-        position = lax.broadcasted_iota(jnp.int32, scores.shape, 1)
-        scores = jnp.where(position < length[b : b + 1, 0:1], scores * scale, -jnp.inf)
-        peak = jnp.maximum(jnp.max(scores, axis=-1, keepdims=True), own_score)
-        past = jnp.exp(scores - peak)
-        own_exp = jnp.exp(own_score - peak)
-        total = jnp.sum(past, axis=-1, keepdims=True) + own_exp
-        past = (past / total).astype(BF16)
-        own_weight = (own_exp / total).astype(BF16).astype(F32)
-        outs.append(nn(past, v_cl[b]) + own_weight * lat_b)
-    mixed_lat = nn(to_dev, join(outs).astype(BF16))
+        q_b = jnp.where(mine[b][:, 0:1], q_lat32, 0.0).astype(BF16)
+        wide_q.append(q_b)
+        turned = pltpu.roll(q_rot, rope * b, 1) if b else q_rot
+        turned = jnp.where(mine[b], turned, 0.0)
+        across = turned if across is None else across + turned
+    across = across[:, 0 : own * rope].astype(BF16)
+    wide_q = jnp.concatenate(wide_q, axis=1)
+    if own * big < lanes:
+        wide_q = join([wide_q, jnp.zeros((lanes - own * big, own * latent), BF16)])
+    depth = v_cl.shape[1] // 2
+    scores = []
+    for part in range(2):
+        cut = slice(part * depth, (part + 1) * depth)
+        keys = jnp.concatenate([v_cl[b, cut, :] for b in range(own)], axis=1)
+        scores.append(nt(keys, wide_q).T[0 : own * big] + nn(across, v_cr[:, cut]))
+    scores = jnp.concatenate(scores, axis=1)
+    position = lax.broadcasted_iota(jnp.int32, scores.shape, 1)
+    scores = jnp.where(position < length[:, 0:1], scores * scale, -jnp.inf)
+    peak = jnp.maximum(jnp.max(scores, axis=-1, keepdims=True), own_score)
+    past = jnp.exp(scores - peak)
+    own_exp = jnp.exp(own_score - peak)
+    total = jnp.sum(past, axis=-1, keepdims=True) + own_exp
+    past = past / total
+    own_weight = (own_exp / total).astype(BF16).astype(F32)
+    past = [jnp.where(mine[b][:, 0:1], past, 0.0).astype(BF16) for b in range(own)]
+    mixed_lat = []
+    for part in range(2):
+        cut = slice(part * latent // 2, (part + 1) * latent // 2)
+        total = None
+        for b in range(own):
+            term = nn(past[b], v_cl[b, :, cut])
+            total = term if total is None else total + term
+        mixed_lat.append(total)
+    mixed_lat = jnp.concatenate(mixed_lat, axis=1)
+    mixed_lat = mixed_lat + own_weight * new_lat_all
     for u in range(T):
         sendo[u] = mixed_lat[R * u : R * (u + 1)].astype(BF16)
     step = tp_exchange(2, lambda peer: sendo.at[peer], recvo)
@@ -373,22 +385,31 @@
     arrive(step)
 
     back = rows_of(recvo, T).astype(BF16)
-    part = None
+    values = []
     for h in range(H):
-        values = nt(back, v_vu[h])
-        values = join(
-            [values[R * u + own * h : R * u + own * (h + 1)] for u in range(T)]
-        ).astype(BF16)
-        term = nn(values, v_wo[h])
-        part = term if part is None else part + term
+        value = nt(back, v_vu[h])
+        values.append(
+            join([value[R * u + own * h : R * u + own * (h + 1)] for u in range(T)])
+        )
+    values = values[0] if H == 1 else jnp.concatenate(values, axis=1)
+    values = values.astype(BF16)
+    wide = v_wo.shape[1] // 2
+    part = jnp.concatenate(
+        [nn(values, v_wo[:, 0:wide]), nn(values, v_wo[:, wide : 2 * wide])], axis=1
+    )
     for u in range(T):
         senda[u] = part[own * u : own * (u + 1)].astype(BF16)
-    after = tokens[...].astype(F32) + tp_scatter(3, senda, half_a, whole_a, recva)
+    step = tp_exchange(3, lambda peer: senda.at[peer], recva)
+    recva[me_t] = senda[me_t]
+    arrive(step)
+    after = tokens[...].astype(F32)
+    for u in range(T):
+        after = after + recva[u].astype(F32)
     agf[me_t] = (after * factor_of(after) * flat(ffn_gain[...])).astype(BF16)
-    finish = tp_gather(4, agf)
+    step = tp_exchange(4, lambda peer: agf.at[me_t], agf)
     for i in range(first_ffn, len(loads)):
         loads[i].wait()
-    finish()
+    arrive(step)
 
     rows32 = rows_of(agf, T)
     rows = rows32.astype(BF16)
@@ -398,16 +419,16 @@
     step = ep_exchange(0, sende, recve)
     recve[me_e] = sende[me_e]
 
-    act = (silu(nt(rows, v_sg[...])) * nt(rows, v_su[...])).astype(BF16)
+    act = (silu(nt(rows, v_s[0])) * nt(rows, v_s[1])).astype(BF16)
     ffn = nn(act, v_sd[...])
     gate = jnp.sum(rows32 * flat(branch_gate[...].astype(F32)), axis=-1, keepdims=True)
     gate = 1.0 / (1.0 + jnp.exp(-gate))
-    act = (silu(nn(rows, v_dg[...])) * nn(rows, v_du[...])).astype(BF16)
+    act = (silu(nn(rows, v_d[0])) * nn(rows, v_d[1])).astype(BF16)
     ffn = ffn + gate * nn(act, v_dd[...])
 
     arrive(step)
     routed = rows_of(recve, EP).astype(BF16)
-    act = (silu(nn(routed, v_eg[...])) * nn(routed, v_eu[...])).astype(BF16)
+    act = (silu(nn(routed, v_e[0])) * nn(routed, v_e[1])).astype(BF16)
     wide = v_ed.shape[1] // 2
     cuts = [slice(0, wide), slice(wide, 2 * wide)]
     steps = []
@@ -467,24 +488,24 @@
     turns = jnp.asarray(np.concatenate([np.cos(angles), np.sin(angles)]), F32)
 
     operands = (
+        tokens,
+        attn_gain.reshape(-1, lanes),
+        lengths,
         turns,
-        tokens,
         route_ids.T,
         route_weights.T,
-        attn_gain.reshape(-1, lanes),
         ffn_gain.reshape(-1, lanes),
         latent_gain.reshape(-1, lanes),
         branch_gate.reshape(-1, lanes),
-        lengths,
         w_query_nope.transpose(1, 2, 0).reshape(H * nope, width),
         w_query_rope.transpose(1, 2, 0).reshape(H * rope, width),
         w_latent_down.T,
         w_key_rope.T,
         cache_latent,
-        cache_rope_key.transpose(0, 2, 1),
+        cache_rope_key.transpose(0, 2, 1).reshape(own * rope, -1),
         w_key_up.transpose(1, 2, 0),
         w_value_up.transpose(1, 2, 0),
-        w_attn_out,
+        w_attn_out.reshape(-1, width),
         shared_gate.T,
         shared_up.T,
         dense_gate,
@@ -497,7 +518,15 @@
     )
     big = operands[9:]
     v_in = pltpu.VMEM((sum(o.shape[0] for o in big[:3]), width), BF16)
-    weights = [v_in] + [pltpu.VMEM(o.shape, BF16) for o in big[3:]]
+    weights = [v_in] + [
+        pltpu.VMEM(shape, BF16)
+        for shape in [o.shape for o in big[3:9]]
+        + [(2,) + o.shape for o in (big[9], big[11])]
+        + [big[13].shape, big[14].shape, (2,) + big[15].shape, big[17].shape]
+    ]
+    small = [
+        (pltpu.SMEM if o is lengths else pltpu.VMEM)(o.shape, o.dtype) for o in operands[:9]
+    ]
     q_width = latent + lanes
 
     def comm(*shape):
@@ -512,39 +541,33 @@
         comm(EP, cap, width), comm(EP, cap, width),
         comm(2, EP, cap, width // 2), comm(2, EP, cap, width // 2),
         comm(2, T, own, width // 2), comm(2, T, own, width // 2),
-        comm(T, own, width), comm(T, own, width),
         pltpu.VMEM((own, lanes), F32),
     ]
-    n_loads = len(big) + own - 1
+    n_loads = 22
     sems = [
         pltpu.SemaphoreType.DMA((n_loads,)),
-        pltpu.SemaphoreType.DMA((7, T)),
-        pltpu.SemaphoreType.DMA((7, T)),
-        pltpu.SemaphoreType.DMA((3, EP)),
-        pltpu.SemaphoreType.DMA((3, EP)),
+        pltpu.SemaphoreType.DMA((7,)),
+        pltpu.SemaphoreType.DMA((7,)),
+        pltpu.SemaphoreType.DMA((3,)),
+        pltpu.SemaphoreType.DMA((3,)),
     ]
     sizes = (T, EP, own, H, nope, rope, latent, cap, (nope + rope) ** (-0.5))
     vmem = pl.BlockSpec(memory_space=pltpu.VMEM)
+    shapes = [((own, width), BF16), ((own, latent), BF16), ((own, rope), BF16)]
     results = pl.pallas_call(
         functools.partial(layer, sizes),
-        out_shape=(
-            jax.ShapeDtypeStruct((own, width), BF16),
-            jax.ShapeDtypeStruct((own, latent), BF16),
-            jax.ShapeDtypeStruct((own, rope), BF16),
-        ),
-        in_specs=[vmem] * 8
-        + [pl.BlockSpec(memory_space=pltpu.SMEM)]
-        + [pl.BlockSpec(memory_space=pl.ANY)] * len(big),
+        out_shape=tuple(pltpu.VMEM(*shape) for shape in shapes),
+        in_specs=[pl.BlockSpec(memory_space=pl.ANY)] * len(operands),
         out_specs=(vmem, vmem, vmem),
-        scratch_shapes=weights + buffers + sems,
+        scratch_shapes=small + weights + buffers + sems,
         compiler_params=pltpu.CompilerParams(collective_id=0, has_side_effects=True),
     )(*operands)
     return pl.pallas_call(
         hand_over,
-        out_shape=tuple(jax.ShapeDtypeStruct(r.shape, r.dtype) for r in results),
+        out_shape=tuple(jax.ShapeDtypeStruct(*shape) for shape in shapes),
         in_specs=[vmem] * 3,
         out_specs=(vmem, vmem, vmem),
-    )(*results)
+    )(*[pltpu.with_memory_space_constraint(r, pltpu.VMEM) for r in results])
 
 
 def solution(mesh):

time: 49.2 us -> 43.8 us (0.89)
  Pallas kernels: 48.3 us -> 42.9 us
    pallas_call x2, Pallas kernels: 48.3 us -> 42.9 us  [the longest x1 42.3 us: local(): pl.pallas_call(functools.partial(layer, sizes), out_shape=tuple((pltpu.VM...]
where the time goes in v1:
time: 43.8 us; the launch traced here: 43.5 us
  Pallas kernels  42.9 us (98%)
  between operations  0.65 us (1%)
    pallas_call x1, Pallas kernels, local(): pl.pallas_call(functools.partial(layer, sizes), out_shape=tuple((pltpu.VM...  42.3 us

profile of v1, /device:TPU:0, one launch (start us, length us, event | category | flops | bytes accessed | tf_op | source)
XLA Modules:
  0.0 43.5 jit_solution(18277720468343593786)
XLA Ops:
  0.6 42.3 %shard_map.274 = (bf16[4,2048]{1,0:T(4,128)(2,1)S(1)}, bf16[4,512]{1,0:T(4,128)(2,1)S(1)}, bf16[4,32]{1,0:T(4,128)(2,1)S(1)}) custom-call(bf16[4,2048]{1,0:T(4,128)(2,1)} %h_tokens.1, f32[16,128]{1,0:T(8,128)} %bitcast.38, s32[4]{0:T(128)} %h_lengths.1, f32[22,128]{1,0:T(8,128)} %constant.2.clone.h_turns, s32[4,32]{1,0:T(4,128)} %bitcast.41, ...), custom_call_target="tpu_custom_call" | custom-call | tf_op jit(solution)/shard_map/pallas_call | solution.py:557
  42.9 0.6 %shard_map.275 = (bf16[4,2048]{1,0:T(4,128)(2,1)}, bf16[4,512]{1,0:T(4,128)(2,1)}, bf16[4,32]{1,0:T(4,128)(2,1)}) custom-call(bf16[4,2048]{1,0:T(4,128)(2,1)S(1)} %get-tuple-element.6.refs_0_, bf16[4,512]{1,0:T(4,128)(2,1)S(1)} %get-tuple-element.7.refs_1_, bf16[4,32]{1,0:T(4,128)(2,1)S(1)} %get-tuple-element.8.refs_2_), custom_call_target="tpu_custom_call" | custom-call | tf_op jit(solution)/shard_map/pallas_call | solution.py:565

commit v2 on v1

--- a/solution.py
+++ b/solution.py
@@ -42,19 +42,14 @@
     return out
 
 
-def far_first(me, chips, cores):
-    chip, core = me // cores, me % cores
+def far_first(chip, chips):
     low = 1 - chip // (chips // 2)
     order = []
     for i in range(chips - 1):
         down = chips - 1 - i
         down = down - (chip - down + chips) // chips
         up = i + (i - chip + chips) // chips
-        to = low * down + (1 - low) * up
-        for turn_core in range(cores):
-            order.append(to * cores + (core + turn_core) % cores)
-    for turn_core in range(1, cores):
-        order.append(chip * cores + (core + turn_core) % cores)
+        order.append(low * down + (1 - low) * up)
     return order
 
 
@@ -77,17 +72,25 @@
     return lax.rsqrt(jnp.mean(values * values, axis=-1, keepdims=True) + epsilon)
 
 
+def in_three(value):
+    lane = lax.broadcasted_iota(jnp.int32, (value.shape[0], lanes), 1)
+    out = jnp.zeros(lane.shape, F32)
+    for i in range(3):
+        part = value.astype(BF16).astype(F32)
+        out = jnp.where(lane == i, part, out)
+        value = value - part
+    return out.astype(BF16)
+
+
+def scaled(halves):
+    half = halves[0].shape[1] - lanes
+    total = jnp.sum(halves[0][:, half:] + halves[1][:, half:], axis=-1, keepdims=True)
+    factor = lax.rsqrt(total / (2 * half) + epsilon)
+    return jnp.concatenate([(h[:, 0:half] * factor).astype(BF16) for h in halves], axis=1)
+
+
 def silu(v):
     return v / (1.0 + jnp.exp(-v))
-
-
-def lane_block(values, column, width):
-    base, offset = column // lanes * lanes, column % lanes
-    block = values[:, base : base + lanes]
-    if offset:
-        block = pltpu.roll(block, lanes - offset, 1)
-    lane = lax.broadcasted_iota(jnp.int32, block.shape, 1)
-    return jnp.where(lane < width, block, 0.0)
 
 
 def turn(values, cosine, sine, half):
@@ -103,10 +106,11 @@
     h_tokens, h_attn_gain, h_lengths, h_turns, h_ids, h_wts, h_ffn_gain, h_latent_gain, h_branch_gate,
     wqn, wqr, wld, wkr, cl, cr, wku, wvu, wo, sg, su, dg, du, sd, dd, eg, eu, ed,
     mixed, newlat, newrope,
-    tokens, attn_gain, lengths, turns, ids, wts, ffn_gain, latent_gain, branch_gate,
+    toks, attn_gain, lengths, turns, ids, wts, ffn_gain, latent_gain, branch_gate,
     v_in, v_kr, v_cl, v_cr, v_ku, v_vu, v_wo, v_s, v_d, v_sd, v_dd, v_e, v_ed,
-    agx, sendq, recvq, sendo, recvo, senda, recva, agf, sende, recve, sendr, recvr, sendf, recvf,
-    kr_pad, w_sem, tp_send, tp_recv, ep_send, ep_recv,
+    agx, sendq, recvq, sendo, recvo, senda, recva, half_after, after, agf, halves,
+    sende, recve, ffn_own, ffn_other, sendr, recvr, sendf, recvf,
+    kr_pad, w_sem, tp_send, tp_recv, ep_send, ep_recv, pair_send, pair_recv,
 ):
     T, EP, own, H, nope, rope, latent, cap, scale = sizes
     group = T * own
@@ -115,35 +119,45 @@
     me_e = lax.axis_index("ep")
     lat_w = wld.shape[0]
 
+    Z = T // 2
+    me_z, me_k = me_t // 2, me_t % 2
+    partner = me_t + 1 - 2 * me_k
+    width = agx.shape[2]
+    half = width // 2
+    chips = far_first(me_z, Z)
+    order = []
+    for z in chips:
+        order += [2 * z + me_k, 2 * z + 1 - me_k]
+    order.append(partner)
+
     barrier = pltpu.get_barrier_semaphore()
-    for k in range(1, T):
-        pl.semaphore_signal(
-            barrier, inc=1, device_id=(me_e, flipped(me_t, k, T)), device_id_type=MESH
-        )
+    for peer in order:
+        pl.semaphore_signal(barrier, inc=1, device_id=(me_e, peer), device_id_type=MESH)
     for k in range(1, EP):
-        pl.semaphore_signal(
-            barrier, inc=1, device_id=(flipped(me_e, k, EP), me_t), device_id_type=MESH
-        )
+        for peer in (me_t, partner):
+            pl.semaphore_signal(
+                barrier, inc=1, device_id=(flipped(me_e, k, EP), peer), device_id_type=MESH
+            )
 
     n_q, n_r = H * nope, H * rope
     groups = [
-        [(h_tokens, tokens)],
+        [(h_tokens, toks.at[me_k])],
         [(h_attn_gain, attn_gain)],
         [
-            (wqn, v_in.at[pl.ds(0, n_q)]),
-            (wqr, v_in.at[pl.ds(n_q, n_r)]),
-            (wld, v_in.at[pl.ds(n_q + n_r, lat_w)]),
+            (wqn, v_in.at[me_k, pl.ds(0, n_q)]),
+            (wqr, v_in.at[me_k, pl.ds(n_q, n_r)]),
+            (wld, v_in.at[me_k, pl.ds(n_q + n_r, lat_w)]),
         ],
         [(wkr, v_kr)],
-        [(wku, v_ku)],
+        [(wku, v_ku.at[me_k])],
         [(h_lengths, lengths)],
         [(h_turns, turns)],
         [(h_ids, ids)],
         [(h_wts, wts)],
         [(cl, v_cl)],
         [(cr, v_cr)],
-        [(wvu, v_vu)],
-        [(wo, v_wo)],
+        [(wvu, v_vu.at[me_k])],
+        [(wo, v_wo.at[me_k])],
         [(h_latent_gain, latent_gain)],
         [(h_ffn_gain, ffn_gain)],
         [(sg, v_s.at[0]), (su, v_s.at[1])],
@@ -154,7 +168,7 @@
         [(eg, v_e.at[0]), (eu, v_e.at[1])],
         [(ed, v_ed)],
     ]
-    wholes = {2: v_in, 15: v_s, 16: v_d, 20: v_e}
+    wholes = {2: v_in.at[me_k], 15: v_s, 16: v_d, 20: v_e}
     first_small, first_cl, first_ffn = 2, 9, 15
     loads = []
     for i, bunch in enumerate(groups):
@@ -167,72 +181,71 @@
 
     sends = []
 
-    order = far_first(me_t, T // 2, 2)
-
-    def tp_exchange(phase, source, target):
-        for peer in order:
-            pltpu.make_async_remote_copy(
-                src_ref=source(peer),
-                dst_ref=target.at[me_t],
-                send_sem=tp_send.at[phase],
-                recv_sem=tp_recv.at[phase],
-                device_id=(me_e, peer),
-                device_id_type=MESH,
-            ).start()
-        blocks = target.at[pl.ds(0, T - 1)]
-        every = pltpu.make_async_remote_copy(
-            src_ref=blocks,
-            dst_ref=blocks,
-            send_sem=tp_send.at[phase],
-            recv_sem=tp_recv.at[phase],
-            device_id=(me_e, order[0]),
+    def remote(source, target, send_sem, recv_sem, e, t):
+        return pltpu.make_async_remote_copy(
+            src_ref=source,
+            dst_ref=target,
+            send_sem=send_sem,
+            recv_sem=recv_sem,
+            device_id=(e, t),
             device_id_type=MESH,
         )
+
+    def whole(blocks, send_sem, recv_sem):
+        every = remote(blocks, blocks, send_sem, recv_sem, me_e, partner)
         sends.append(every)
         return every
 
+    def tp_exchange(phase, source, target):
+        sems = tp_send.at[phase], tp_recv.at[phase]
+        for peer in order:
+            remote(source(peer), target.at[me_t], *sems, me_e, peer).start()
+        return whole(target.at[pl.ds(0, T - 1)], *sems)
+
+    def chip_exchange(phase, source, target, core):
+        sems = tp_send.at[phase], tp_recv.at[phase]
+        for z in chips:
+            remote(source(z), target.at[me_z], *sems, me_e, 2 * z + core).start()
+        return whole(target.at[pl.ds(0, Z - 1)], *sems)
+
     def ep_exchange(phase, source, target):
+        sems = ep_send.at[phase], ep_recv.at[phase]
         for k in range(EP - 1, 0, -1):
             peer = flipped(me_e, k, EP)
-            pltpu.make_async_remote_copy(
-                src_ref=source.at[peer],
-                dst_ref=target.at[me_e],
-                send_sem=ep_send.at[phase],
-                recv_sem=ep_recv.at[phase],
-                device_id=(peer, me_t),
-                device_id_type=MESH,
-            ).start()
-        blocks = target.at[pl.ds(0, EP - 1)]
-        every = pltpu.make_async_remote_copy(
-            src_ref=blocks,
-            dst_ref=blocks,
-            send_sem=ep_send.at[phase],
-            recv_sem=ep_recv.at[phase],
-            device_id=(flipped(me_e, 1, EP), me_t),
-            device_id_type=MESH,
-        )
-        sends.append(every)
-        return every
+            for c, t in ((me_k, me_t), (1 - me_k, partner)):
+                remote(source.at[2 * peer + c], target.at[2 * me_e + me_k], *sems, peer, t).start()
+        mine = 2 * me_e + me_k
+        remote(source.at[2 * me_e + 1 - me_k], target.at[mine], *sems, me_e, partner).start()
+        target[mine] = source[mine]
+        return whole(target.at[pl.ds(0, 2 * EP - 1)], *sems)
+
+    def pair_copy(i, source, target):
+        copy = remote(source, target, pair_send.at[i], pair_recv.at[i], me_e, partner)
+        copy.start()
+        sends.append(copy)
+        return copy
 
     def arrive(step):
         step.wait_recv()
 
     for i in range(first_small):
         loads[i].wait()
-    x = tokens[...].astype(F32)
+    x = toks[me_k].astype(F32)
     normed = (x * factor_of(x) * flat(attn_gain[...])).astype(BF16)
-    agx[me_t] = normed
-    pl.semaphore_wait(barrier, T - 1 + EP - 1)
-    step = tp_exchange(0, lambda peer: agx.at[me_t], agx)
+    agx[me_z] = normed
+    pl.semaphore_wait(barrier, T - 1 + 2 * (EP - 1))
+    step = chip_exchange(0, lambda z: agx.at[me_z], agx, 1 - me_k)
     for i in range(first_small, first_cl):
         loads[i].wait()
-
-    slots = EP * cap
+    early = [
+        pair_copy(6, v_in.at[me_k], v_in.at[me_k]),
+        pair_copy(7, v_ku.at[me_k], v_ku.at[me_k]),
+    ]
+
+    slots = EP * 2 * cap
     slot = lax.broadcasted_iota(jnp.int32, (slots, group), 0)
-    block = jnp.zeros((slots, group), jnp.int32)
-    for j in range(1, EP):
-        block = block + jnp.where(slot >= j * cap, 1, 0)
-    expert = block * T + me_t
+    block = slot // cap
+    expert = block // 2 * T + block % 2 + 2 * me_z
     place = (slot - block * cap).astype(F32)
     hit = jnp.zeros((slots, group), F32)
     weight = jnp.zeros((slots, group), F32)
@@ -286,30 +299,39 @@
     new_rope = turn(kr_pad[...], cosine, sine, rope // 2).astype(BF16)
     newrope[...] = new_rope[:, 0:rope]
 
+    for copy in early:
+        arrive(copy)
     arrive(step)
-    rows = rows_of(agx, T).astype(BF16)
-    wide = v_in.shape[0] // 2
-    proj = jnp.concatenate(
-        [nt(rows, v_in[0:wide, :]), nt(rows, v_in[wide : 2 * wide, :])], axis=1
-    )
-    q_lat = [
-        nn(lane_block(proj, h * nope, nope)[:, 0:nope].astype(BF16), v_ku[h]) for h in range(H)
+    rows = rows_of(agx, Z).astype(BF16)
+    count = rows.shape[0]
+    lane = lax.broadcasted_iota(jnp.int32, (count, n_q), 1) // nope
+    spare = jnp.zeros((lanes - rope - lat_w, count), F32)
+    q_lat, q_rope = [], []
+    projected = [nt(v_in[c], rows) for c in range(2)]
+    for c, proj in enumerate(projected):
+        every = proj[0:n_q].T
+        every = join([jnp.where(lane == h, every, 0.0) for h in range(H)]).astype(BF16)
+        every = nn(every, join([v_ku[c, h] for h in range(H)]))
+        q_lat += [every[count * h : count * (h + 1)] for h in range(H)]
+        for h in range(H):
+            top = n_q + h * rope
+            q_rope.append(join([proj[top : top + rope], spare, proj[n_q + n_r :]]).T)
+    for z in range(Z):
+        cut = slice(own * z, own * (z + 1))
+        sendq[z, :, 0:latent] = join([q[cut] for q in q_lat]).astype(BF16)
+        sendq[z, :, latent : latent + lanes] = join([q[cut] for q in q_rope]).astype(BF16)
+    step = chip_exchange(1, lambda z: sendq.at[z], recvq, 1 - me_k)
+    recvq[me_z] = sendq[me_z]
+    shared = [
+        pair_copy(0, toks.at[me_k], toks.at[me_k]),
+        pair_copy(1, wvu, v_vu.at[me_k]),
+        pair_copy(2, wo, v_wo.at[me_k]),
     ]
-    q_rope = [lane_block(proj, n_q + h * rope, rope) for h in range(H)]
-    lat_part = pltpu.roll(lane_block(proj, n_q + n_r, lat_w), lanes - lat_w, 1)
-    for u in range(T):
-        cut = slice(own * u, own * (u + 1))
-        sendq[u, :, 0:latent] = join([q[cut] for q in q_lat]).astype(BF16)
-        sendq[u, :, latent : latent + lanes] = join(
-            [q[cut] + lat_part[cut] for q in q_rope]
-        ).astype(BF16)
-    step = tp_exchange(1, lambda peer: sendq.at[peer], recvq)
-    recvq[me_t] = sendq[me_t]
     for i in range(first_cl, first_ffn):
         loads[i].wait()
     arrive(step)
 
-    queries = rows_of(recvq, T)
+    queries = rows_of(recvq, Z)
     per = lanes // lat_w
     lane = lax.broadcasted_iota(jnp.int32, (own, lanes), 1)
     blocks = []
@@ -350,14 +372,12 @@
         across = turned if across is None else across + turned
     across = across[:, 0 : own * rope].astype(BF16)
     wide_q = jnp.concatenate(wide_q, axis=1)
-    if own * big < lanes:
-        wide_q = join([wide_q, jnp.zeros((lanes - own * big, own * latent), BF16)])
     depth = v_cl.shape[1] // 2
     scores = []
     for part in range(2):
         cut = slice(part * depth, (part + 1) * depth)
         keys = jnp.concatenate([v_cl[b, cut, :] for b in range(own)], axis=1)
-        scores.append(nt(keys, wide_q).T[0 : own * big] + nn(across, v_cr[:, cut]))
+        scores.append(nt(keys, wide_q).T + nn(across, v_cr[:, cut]))
     scores = jnp.concatenate(scores, axis=1)
     position = lax.broadcasted_iota(jnp.int32, scores.shape, 1)
     scores = jnp.where(position < length[:, 0:1], scores * scale, -jnp.inf)
@@ -378,47 +398,69 @@
         mixed_lat.append(total)
     mixed_lat = jnp.concatenate(mixed_lat, axis=1)
     mixed_lat = mixed_lat + own_weight * new_lat_all
-    for u in range(T):
-        sendo[u] = mixed_lat[R * u : R * (u + 1)].astype(BF16)
-    step = tp_exchange(2, lambda peer: sendo.at[peer], recvo)
-    recvo[me_t] = sendo[me_t]
+    for z in range(Z):
+        sendo[z] = mixed_lat[2 * R * z : 2 * R * (z + 1)].astype(BF16)
+    step = chip_exchange(2, lambda z: sendo.at[z], recvo, 1 - me_k)
+    recvo[me_z] = sendo[me_z]
+    for copy in shared:
+        arrive(copy)
     arrive(step)
 
-    back = rows_of(recvo, T).astype(BF16)
+    back = rows_of(recvo, Z).astype(BF16)
+    value = nt(back, join([v_vu[0], v_vu[1]]))
+    heads = 2 * H
+    vhead = value.shape[1] // heads
+    at_head = lax.broadcasted_iota(jnp.int32, value.shape, 0) // own % heads
+    of_head = lax.broadcasted_iota(jnp.int32, value.shape, 1) // vhead
+    value = jnp.where(at_head == of_head, value, 0.0)
     values = []
-    for h in range(H):
-        value = nt(back, v_vu[h])
-        values.append(
-            join([value[R * u + own * h : R * u + own * (h + 1)] for u in range(T)])
-        )
-    values = values[0] if H == 1 else jnp.concatenate(values, axis=1)
-    values = values.astype(BF16)
-    wide = v_wo.shape[1] // 2
-    part = jnp.concatenate(
-        [nn(values, v_wo[:, 0:wide]), nn(values, v_wo[:, wide : 2 * wide])], axis=1
-    )
-    for u in range(T):
-        senda[u] = part[own * u : own * (u + 1)].astype(BF16)
+    for z in range(Z):
+        total = None
+        for q in range(heads):
+            top = own * (heads * z + q)
+            term = value[top : top + own]
+            total = term if total is None else total + term
+        values.append(total)
+    values = join(values).astype(BF16)
+    for c in range(2):
+        cut = slice(c * half, (c + 1) * half)
+        part = nn(values, join([v_wo[0, :, cut], v_wo[1, :, cut]]))
+        for z in range(Z):
+            senda[2 * z + c] = part[own * z : own * (z + 1)].astype(BF16)
     step = tp_exchange(3, lambda peer: senda.at[peer], recva)
     recva[me_t] = senda[me_t]
     arrive(step)
-    after = tokens[...].astype(F32)
-    for u in range(T):
-        after = after + recva[u].astype(F32)
-    agf[me_t] = (after * factor_of(after) * flat(ffn_gain[...])).astype(BF16)
-    step = tp_exchange(4, lambda peer: agf.at[me_t], agf)
+    here = pl.ds(pl.multiple_of(me_k * half, lanes), half)
+    eight = []
+    for c in range(2):
+        total = toks[c, :, here].astype(F32) + recva[2 * me_z + c].astype(F32)
+        for z in chips:
+            total = total + recva[2 * z + 1 - c].astype(F32)
+        half_after[c] = total
+        eight.append(total)
+    eight = join(eight)
+    tiles = half // lanes
+    gain = jnp.concatenate(
+        [ffn_gain[pl.ds(me_k * tiles + i, 1), :] for i in range(tiles)], axis=1
+    )
+    agf[me_z, :, 0:half] = (eight * gain).astype(BF16)
+    agf[me_z, :, half:] = in_three(jnp.sum(eight * eight, axis=-1, keepdims=True))
+    step = chip_exchange(4, lambda z: agf.at[me_z], agf, me_k)
+    after_copy = pair_copy(3, half_after.at[1 - me_k], after.at[me_k])
+    after[me_k] = half_after[me_k]
     for i in range(first_ffn, len(loads)):
         loads[i].wait()
     arrive(step)
 
-    rows32 = rows_of(agf, T)
-    rows = rows32.astype(BF16)
-    outgoing = nn(dispatch, rows)
-    for j in range(EP):
+    unscaled = rows_of(agf, Z).astype(BF16)
+    halves[me_k] = unscaled
+    outgoing = nn(dispatch, unscaled)
+    for j in range(2 * EP):
         sende[j] = outgoing[cap * j : cap * (j + 1)].astype(BF16)
     step = ep_exchange(0, sende, recve)
-    recve[me_e] = sende[me_e]
-
+    arrive(pair_copy(4, halves.at[me_k], halves.at[me_k]))
+    rows = scaled([halves[c].astype(F32) for c in range(2)])
+    rows32 = rows.astype(F32)
     act = (silu(nt(rows, v_s[0])) * nt(rows, v_s[1])).astype(BF16)
     ffn = nn(act, v_sd[...])
     gate = jnp.sum(rows32 * flat(branch_gate[...].astype(F32)), axis=-1, keepdims=True)
@@ -426,33 +468,44 @@
     act = (silu(nn(rows, v_d[0])) * nn(rows, v_d[1])).astype(BF16)
     ffn = ffn + gate * nn(act, v_dd[...])
 
+    for c in range(2):
+        ffn_own[c] = ffn[:, c * half : (c + 1) * half]
+    ffn_copy = pair_copy(5, ffn_own.at[1 - me_k], ffn_other)
+
     arrive(step)
-    routed = rows_of(recve, EP).astype(BF16)
+    routed = scaled([join([recve[2 * j + c].astype(F32) for j in range(EP)]) for c in range(2)])
     act = (silu(nn(routed, v_e[0])) * nn(routed, v_e[1])).astype(BF16)
-    wide = v_ed.shape[1] // 2
-    cuts = [slice(0, wide), slice(wide, 2 * wide)]
+    pieces = sendr.shape[0]
+    wide = half // pieces
     steps = []
-    for n, cut in enumerate(cuts):
-        result = nn(act, v_ed[:, cut])
-        for j in range(EP):
-            sendr[n, j] = result[cap * j : cap * (j + 1)].astype(BF16)
+    for n in range(pieces):
+        for c in range(2):
+            base = c * half + n * wide
+            result = nn(act, v_ed[:, base : base + wide])
+            for j in range(EP):
+                sendr[n, 2 * j + c] = result[cap * j : cap * (j + 1)].astype(BF16)
         steps.append(ep_exchange(1 + n, sendr.at[n], recvr.at[n]))
-        recvr[n, me_e] = sendr[n, me_e]
+    arrive(ffn_copy)
+    arrive(after_copy)
+    ffn = ffn_own[me_k] + ffn_other[...]
     last = []
-    for n, cut in enumerate(cuts):
+    for n in range(pieces):
         arrive(steps[n])
-        returned = rows_of(recvr.at[n], EP).astype(BF16)
-        part = ffn[:, cut] + (tn(weight_hi, returned) + tn(weight_lo, returned))
+        returned = rows_of(recvr.at[n], 2 * EP).astype(BF16)
+        part = ffn[:, n * wide : (n + 1) * wide]
+        part = part + (tn(weight_hi, returned) + tn(weight_lo, returned))
         for u in range(T):
             sendf[n, u] = part[own * u : own * (u + 1)].astype(BF16)
         last.append(tp_exchange(5 + n, lambda peer: sendf.at[n, peer], recvf.at[n]))
         recvf[n, me_t] = sendf[n, me_t]
-    for n, cut in enumerate(cuts):
+    for n in range(pieces):
         arrive(last[n])
-        part = after[:, cut]
-        for u in range(T):
-            part = part + recvf[n, u].astype(F32)
-        mixed[:, cut] = part.astype(BF16)
+        for c in range(2):
+            part = after[c, :, n * wide : (n + 1) * wide]
+            for z in range(Z):
+                part = part + recvf[n, 2 * z + c].astype(F32)
+            base = c * half + n * wide
+            mixed[:, base : base + wide] = part.astype(BF16)
     for c in sends:
         c.wait_send()
 
@@ -504,7 +557,7 @@
         cache_latent,
         cache_rope_key.transpose(0, 2, 1).reshape(own * rope, -1),
         w_key_up.transpose(1, 2, 0),
-        w_value_up.transpose(1, 2, 0),
+        w_value_up.transpose(1, 2, 0).reshape(-1, latent),
         w_attn_out.reshape(-1, width),
         shared_gate.T,
         shared_up.T,
@@ -517,30 +570,35 @@
         expert_down[0],
     )
     big = operands[9:]
-    v_in = pltpu.VMEM((sum(o.shape[0] for o in big[:3]), width), BF16)
+    v_in = pltpu.VMEM((2, sum(o.shape[0] for o in big[:3]), width), BF16)
+    pair = (2,)
     weights = [v_in] + [
         pltpu.VMEM(shape, BF16)
-        for shape in [o.shape for o in big[3:9]]
-        + [(2,) + o.shape for o in (big[9], big[11])]
-        + [big[13].shape, big[14].shape, (2,) + big[15].shape, big[17].shape]
+        for shape in [o.shape for o in big[3:6]]
+        + [pair + o.shape for o in (big[6], big[7], big[8], big[9], big[11])]
+        + [big[13].shape, big[14].shape, pair + big[15].shape, big[17].shape]
     ]
-    small = [
-        (pltpu.SMEM if o is lengths else pltpu.VMEM)(o.shape, o.dtype) for o in operands[:9]
+    small = [pltpu.VMEM((2, own, width), BF16)] + [
+        (pltpu.SMEM if o is lengths else pltpu.VMEM)(o.shape, o.dtype) for o in operands[1:9]
     ]
     q_width = latent + lanes
 
     def comm(*shape):
         return pltpu.VMEM(shape, BF16)
 
+    half, chips, group, pieces = width // 2, T // 2, T * own, 2
     buffers = [
-        comm(T, own, width),
-        comm(T, R, q_width), comm(T, R, q_width),
-        comm(T, R, latent), comm(T, R, latent),
-        comm(T, own, width), comm(T, own, width),
-        comm(T, own, width),
-        comm(EP, cap, width), comm(EP, cap, width),
-        comm(2, EP, cap, width // 2), comm(2, EP, cap, width // 2),
-        comm(2, T, own, width // 2), comm(2, T, own, width // 2),
+        comm(chips, own, width),
+        comm(chips, 2 * R, q_width), comm(chips, 2 * R, q_width),
+        comm(chips, 2 * R, latent), comm(chips, 2 * R, latent),
+        comm(T, own, half), comm(T, own, half),
+        pltpu.VMEM((2, own, half), F32), pltpu.VMEM((2, own, half), F32),
+        comm(chips, 2 * own, half + lanes),
+        comm(2, group, half + lanes),
+        comm(2 * EP, cap, half + lanes), comm(2 * EP, cap, half + lanes),
+        pltpu.VMEM((2, group, half), F32), pltpu.VMEM((group, half), F32),
+        comm(pieces, 2 * EP, cap, half // pieces), comm(pieces, 2 * EP, cap, half // pieces),
+        comm(pieces, T, own, half // pieces), comm(pieces, T, own, half // pieces),
         pltpu.VMEM((own, lanes), F32),
     ]
     n_loads = 22
@@ -550,6 +608,8 @@
         pltpu.SemaphoreType.DMA((7,)),
         pltpu.SemaphoreType.DMA((3,)),
         pltpu.SemaphoreType.DMA((3,)),
+        pltpu.SemaphoreType.DMA((8,)),
+        pltpu.SemaphoreType.DMA((8,)),
     ]
     sizes = (T, EP, own, H, nope, rope, latent, cap, (nope + rope) ** (-0.5))
     vmem = pl.BlockSpec(memory_space=pltpu.VMEM)

time: 43.8 us -> 40.7 us (0.929)
  Pallas kernels: 42.9 us -> 39.8 us
    pallas_call x1, Pallas kernels: 42.3 us -> 39.2 us  [local(): pl.pallas_call(functools.partial(layer, sizes), out_shape=tuple((pltpu.VM...]
where the time goes in v2:
time: 40.7 us; the launch traced here: 40.5 us
  Pallas kernels  39.8 us (98%)
  between operations  0.65 us (2%)
    pallas_call x1, Pallas kernels, local(): pl.pallas_call(functools.partial(layer, sizes), out_shape=tuple((pltpu.VM...  39.2 us

profile of v2, /device:TPU:0, one launch (start us, length us, event | category | flops | bytes accessed | tf_op | source)
XLA Modules:
  0.0 40.5 jit_solution(5218673437717883335)
XLA Ops:
  0.6 39.2 %shard_map.274 = (bf16[4,2048]{1,0:T(4,128)(2,1)S(1)}, bf16[4,512]{1,0:T(4,128)(2,1)S(1)}, bf16[4,32]{1,0:T(4,128)(2,1)S(1)}) custom-call(bf16[4,2048]{1,0:T(4,128)(2,1)} %h_tokens.1, f32[16,128]{1,0:T(8,128)} %bitcast.40, s32[4]{0:T(128)} %h_lengths.1, f32[22,128]{1,0:T(8,128)} %constant.2.clone.h_turns, s32[4,32]{1,0:T(4,128)} %bitcast.43, ...), custom_call_target="tpu_custom_call" | custom-call | tf_op jit(solution)/shard_map/pallas_call | solution.py:617
  39.9 0.6 %shard_map.275 = (bf16[4,2048]{1,0:T(4,128)(2,1)}, bf16[4,512]{1,0:T(4,128)(2,1)}, bf16[4,32]{1,0:T(4,128)(2,1)}) custom-call(bf16[4,2048]{1,0:T(4,128)(2,1)S(1)} %get-tuple-element.6.refs_0_, bf16[4,512]{1,0:T(4,128)(2,1)S(1)} %get-tuple-element.7.refs_1_, bf16[4,32]{1,0:T(4,128)(2,1)S(1)} %get-tuple-element.8.refs_2_), custom_call_target="tpu_custom_call" | custom-call | tf_op jit(solution)/shard_map/pallas_call | solution.py:625

commit v3 on v2

--- a/solution.py
+++ b/solution.py
@@ -72,23 +72,6 @@
     return lax.rsqrt(jnp.mean(values * values, axis=-1, keepdims=True) + epsilon)
 
 
-def in_three(value):
-    lane = lax.broadcasted_iota(jnp.int32, (value.shape[0], lanes), 1)
-    out = jnp.zeros(lane.shape, F32)
-    for i in range(3):
-        part = value.astype(BF16).astype(F32)
-        out = jnp.where(lane == i, part, out)
-        value = value - part
-    return out.astype(BF16)
-
-
-def scaled(halves):
-    half = halves[0].shape[1] - lanes
-    total = jnp.sum(halves[0][:, half:] + halves[1][:, half:], axis=-1, keepdims=True)
-    factor = lax.rsqrt(total / (2 * half) + epsilon)
-    return jnp.concatenate([(h[:, 0:half] * factor).astype(BF16) for h in halves], axis=1)
-
-
 def silu(v):
     return v / (1.0 + jnp.exp(-v))
 
@@ -106,11 +89,11 @@
     h_tokens, h_attn_gain, h_lengths, h_turns, h_ids, h_wts, h_ffn_gain, h_latent_gain, h_branch_gate,
     wqn, wqr, wld, wkr, cl, cr, wku, wvu, wo, sg, su, dg, du, sd, dd, eg, eu, ed,
     mixed, newlat, newrope,
-    toks, attn_gain, lengths, turns, ids, wts, ffn_gain, latent_gain, branch_gate,
+    tokens, attn_gain, lengths, turns, ids, wts, ffn_gain, latent_gain, branch_gate,
     v_in, v_kr, v_cl, v_cr, v_ku, v_vu, v_wo, v_s, v_d, v_sd, v_dd, v_e, v_ed,
-    agx, sendq, recvq, sendo, recvo, senda, recva, half_after, after, agf, halves,
+    agx, sendq, recvq, sendo, recvo, senda, recva, sendg, agf, halves,
     sende, recve, ffn_own, ffn_other, sendr, recvr, sendf, recvf,
-    kr_pad, w_sem, tp_send, tp_recv, ep_send, ep_recv, pair_send, pair_recv,
+    kr_pad, by_row, v_it, v_ct, w_sem, tp_send, tp_recv, ep_send, ep_recv, pair_send, pair_recv,
 ):
     T, EP, own, H, nope, rope, latent, cap, scale = sizes
     group = T * own
@@ -141,12 +124,12 @@
 
     n_q, n_r = H * nope, H * rope
     groups = [
-        [(h_tokens, toks.at[me_k])],
+        [(h_tokens, tokens)],
         [(h_attn_gain, attn_gain)],
         [
-            (wqn, v_in.at[me_k, pl.ds(0, n_q)]),
-            (wqr, v_in.at[me_k, pl.ds(n_q, n_r)]),
-            (wld, v_in.at[me_k, pl.ds(n_q + n_r, lat_w)]),
+            (wqn, v_in.at[pl.ds(0, n_q)]),
+            (wqr, v_in.at[pl.ds(n_q, n_r)]),
+            (wld, v_in.at[pl.ds(n_q + n_r, lat_w)]),
         ],
         [(wkr, v_kr)],
         [(wku, v_ku.at[me_k])],
@@ -168,7 +151,7 @@
         [(eg, v_e.at[0]), (eu, v_e.at[1])],
         [(ed, v_ed)],
     ]
-    wholes = {2: v_in.at[me_k], 15: v_s, 16: v_d, 20: v_e}
+    wholes = {2: v_in, 15: v_s, 16: v_d, 20: v_e}
     first_small, first_cl, first_ffn = 2, 9, 15
     loads = []
     for i, bunch in enumerate(groups):
@@ -230,16 +213,25 @@
 
     for i in range(first_small):
         loads[i].wait()
-    x = toks[me_k].astype(F32)
+    x = tokens[...].astype(F32)
     normed = (x * factor_of(x) * flat(attn_gain[...])).astype(BF16)
     agx[me_z] = normed
+    loads[2].wait()
+    strip = 2 * lanes
+
+    def turn_weights(i, carry):
+        at = pl.ds(pl.multiple_of(i * strip, strip), strip)
+        v_it[me_k, at, :] = v_in[:, at].T
+        return carry
+
+    lax.fori_loop(0, width // strip, turn_weights, 0)
     pl.semaphore_wait(barrier, T - 1 + 2 * (EP - 1))
     step = chip_exchange(0, lambda z: agx.at[me_z], agx, 1 - me_k)
-    for i in range(first_small, first_cl):
+    for i in range(first_small + 1, first_cl):
         loads[i].wait()
     early = [
-        pair_copy(6, v_in.at[me_k], v_in.at[me_k]),
-        pair_copy(7, v_ku.at[me_k], v_ku.at[me_k]),
+        pair_copy(4, v_it.at[me_k], v_it.at[me_k]),
+        pair_copy(5, v_ku.at[me_k], v_ku.at[me_k]),
     ]
 
     slots = EP * 2 * cap
@@ -286,14 +278,10 @@
     cosine = jnp.where(live, cosine, 0.0)
     sine = jnp.where(live, sine, 0.0)
     big = T * H
-    seq = lax.broadcasted_iota(jnp.int32, (own * big, lanes), 0) % own
-
-    def tiled(values):
-        return join([values] * big)
-
+    seq = lax.broadcasted_iota(jnp.int32, (own * big, lanes), 0) // big
     mine = [seq == b for b in range(own)]
-    length = tiled(length)
-    cosines, sines = tiled(cosine), tiled(sine)
+    length = spread(length, big)
+    cosines, sines = spread(cosine, big), spread(sine, big)
     kr_pad[...] = jnp.zeros_like(kr_pad)
     kr_pad[:, 0:rope] = nt(normed, v_kr[...])
     new_rope = turn(kr_pad[...], cosine, sine, rope // 2).astype(BF16)
@@ -304,32 +292,44 @@
     arrive(step)
     rows = rows_of(agx, Z).astype(BF16)
     count = rows.shape[0]
-    lane = lax.broadcasted_iota(jnp.int32, (count, n_q), 1) // nope
-    spare = jnp.zeros((lanes - rope - lat_w, count), F32)
+    of_head = lax.broadcasted_iota(jnp.int32, (count, n_q), 1) // nope
+    lane = lax.broadcasted_iota(jnp.int32, (count, lanes), 1)
     q_lat, q_rope = [], []
-    projected = [nt(v_in[c], rows) for c in range(2)]
+    projected = [nn(rows, v_it[c]) for c in range(2)]
     for c, proj in enumerate(projected):
-        every = proj[0:n_q].T
-        every = join([jnp.where(lane == h, every, 0.0) for h in range(H)]).astype(BF16)
-        every = nn(every, join([v_ku[c, h] for h in range(H)]))
+        every = join([jnp.where(of_head == h, proj[:, 0:n_q], 0.0) for h in range(H)])
+        every = nn(every.astype(BF16), join([v_ku[c, h] for h in range(H)]))
         q_lat += [every[count * h : count * (h + 1)] for h in range(H)]
+        tail = proj[:, proj.shape[1] - lanes :]
+        lat_part = jnp.where(lane >= lanes - lat_w, tail, 0.0)
         for h in range(H):
-            top = n_q + h * rope
-            q_rope.append(join([proj[top : top + rope], spare, proj[n_q + n_r :]]).T)
+            offset = n_q + h * rope - (proj.shape[1] - lanes)
+            piece = pltpu.roll(tail, lanes - offset, 1) if offset else tail
+            q_rope.append(jnp.where(lane < rope, piece, lat_part))
     for z in range(Z):
         cut = slice(own * z, own * (z + 1))
         sendq[z, :, 0:latent] = join([q[cut] for q in q_lat]).astype(BF16)
         sendq[z, :, latent : latent + lanes] = join([q[cut] for q in q_rope]).astype(BF16)
     step = chip_exchange(1, lambda z: sendq.at[z], recvq, 1 - me_k)
     recvq[me_z] = sendq[me_z]
-    shared = [
-        pair_copy(0, toks.at[me_k], toks.at[me_k]),
-        pair_copy(1, wvu, v_vu.at[me_k]),
-        pair_copy(2, wo, v_wo.at[me_k]),
-    ]
     for i in range(first_cl, first_ffn):
         loads[i].wait()
+
+    per_step = 256
+
+    def turn_keys(i, carry):
+        b = i // (v_cl.shape[1] // per_step)
+        at = pl.ds(pl.multiple_of(i % (v_cl.shape[1] // per_step) * per_step, lanes), per_step)
+        v_ct[b, :, at] = v_cl[b, at, :].T
+        return carry
+
+    lax.fori_loop(0, own * (v_cl.shape[1] // per_step), turn_keys, 0)
+
     arrive(step)
+    shared = [
+        pair_copy(0, v_vu.at[me_k], v_vu.at[me_k]),
+        pair_copy(1, v_wo.at[me_k], v_wo.at[me_k]),
+    ]
 
     queries = rows_of(recvq, Z)
     per = lanes // lat_w
@@ -348,6 +348,16 @@
     new_latent = (raw * factor_of(raw) * flat(latent_gain[...])).astype(BF16)
     newlat[...] = new_latent
     new_lat32, new_rope32 = new_latent.astype(F32), new_rope.astype(F32)
+    tiles = by_row.shape[0]
+    for i in range(tiles):
+        by_row[i] = queries[:, lanes * i : lanes * (i + 1)]
+    queries = jnp.concatenate(
+        [
+            join([by_row[i, pl.ds(b, big, stride=own), :] for b in range(own)])
+            for i in range(tiles)
+        ],
+        axis=1,
+    )
     q_rot = turn(
         jnp.where(
             lax.broadcasted_iota(jnp.int32, (own * big, lanes), 1) < rope, queries[:, latent:], 0.0
@@ -357,47 +367,46 @@
         rope // 2,
     ).astype(BF16).astype(F32)
     q_lat32 = queries[:, 0:latent]
-    new_lat_all = tiled(new_lat32)
+    new_lat_all = spread(new_lat32, big)
     own_score = (
         jnp.sum(q_lat32 * new_lat_all, axis=-1, keepdims=True)
-        + jnp.sum(q_rot * tiled(new_rope32), axis=-1, keepdims=True)
+        + jnp.sum(q_rot * spread(new_rope32, big), axis=-1, keepdims=True)
     ) * scale
     across = None
-    wide_q = []
+    q_lat16 = q_lat32.astype(BF16)
     for b in range(own):
-        q_b = jnp.where(mine[b][:, 0:1], q_lat32, 0.0).astype(BF16)
-        wide_q.append(q_b)
         turned = pltpu.roll(q_rot, rope * b, 1) if b else q_rot
         turned = jnp.where(mine[b], turned, 0.0)
         across = turned if across is None else across + turned
     across = across[:, 0 : own * rope].astype(BF16)
-    wide_q = jnp.concatenate(wide_q, axis=1)
     depth = v_cl.shape[1] // 2
     scores = []
     for part in range(2):
         cut = slice(part * depth, (part + 1) * depth)
-        keys = jnp.concatenate([v_cl[b, cut, :] for b in range(own)], axis=1)
-        scores.append(nt(keys, wide_q).T + nn(across, v_cr[:, cut]))
+        part = [nn(q_lat16[big * b : big * (b + 1)], v_ct[b, :, cut]) for b in range(own)]
+        scores.append(join(part) + nn(across, v_cr[:, cut]))
     scores = jnp.concatenate(scores, axis=1)
     position = lax.broadcasted_iota(jnp.int32, scores.shape, 1)
     scores = jnp.where(position < length[:, 0:1], scores * scale, -jnp.inf)
     peak = jnp.maximum(jnp.max(scores, axis=-1, keepdims=True), own_score)
     past = jnp.exp(scores - peak)
     own_exp = jnp.exp(own_score - peak)
-    total = jnp.sum(past, axis=-1, keepdims=True) + own_exp
-    past = past / total
-    own_weight = (own_exp / total).astype(BF16).astype(F32)
-    past = [jnp.where(mine[b][:, 0:1], past, 0.0).astype(BF16) for b in range(own)]
+    weights = jnp.sum(past, axis=-1, keepdims=True) + own_exp
+    past = past.astype(BF16)
     mixed_lat = []
     for part in range(2):
         cut = slice(part * latent // 2, (part + 1) * latent // 2)
-        total = None
+        mixed_lat.append(
+            join([nn(past[big * b : big * (b + 1)], v_cl[b, :, cut]) for b in range(own)])
+        )
+    mixed_lat = jnp.concatenate(mixed_lat, axis=1)
+    mixed_lat = (mixed_lat + own_exp * new_lat_all) / weights
+    tiles = latent // lanes
+    for i in range(tiles):
         for b in range(own):
-            term = nn(past[b], v_cl[b, :, cut])
-            total = term if total is None else total + term
-        mixed_lat.append(total)
-    mixed_lat = jnp.concatenate(mixed_lat, axis=1)
-    mixed_lat = mixed_lat + own_weight * new_lat_all
+            block = mixed_lat[big * b : big * (b + 1), lanes * i : lanes * (i + 1)]
+            by_row[i, pl.ds(b, big, stride=own), :] = block
+    mixed_lat = jnp.concatenate([by_row[i] for i in range(tiles)], axis=1)
     for z in range(Z):
         sendo[z] = mixed_lat[2 * R * z : 2 * R * (z + 1)].astype(BF16)
     step = chip_exchange(2, lambda z: sendo.at[z], recvo, 1 - me_k)
@@ -407,7 +416,7 @@
     arrive(step)
 
     back = rows_of(recvo, Z).astype(BF16)
-    value = nt(back, join([v_vu[0], v_vu[1]]))
+    value = jnp.concatenate([nt(back, v_vu[c]) for c in range(2)], axis=1)
     heads = 2 * H
     vhead = value.shape[1] // heads
     at_head = lax.broadcasted_iota(jnp.int32, value.shape, 0) // own % heads
@@ -426,40 +435,30 @@
         cut = slice(c * half, (c + 1) * half)
         part = nn(values, join([v_wo[0, :, cut], v_wo[1, :, cut]]))
         for z in range(Z):
-            senda[2 * z + c] = part[own * z : own * (z + 1)].astype(BF16)
-    step = tp_exchange(3, lambda peer: senda.at[peer], recva)
-    recva[me_t] = senda[me_t]
+            senda[z, :, cut] = part[own * z : own * (z + 1)].astype(BF16)
+    step = chip_exchange(3, lambda z: senda.at[z], recva, 1 - me_k)
+    recva[me_z] = senda[me_z]
     arrive(step)
-    here = pl.ds(pl.multiple_of(me_k * half, lanes), half)
-    eight = []
+    after = tokens[...].astype(F32)
+    for z in range(Z):
+        after = after + recva[z].astype(F32)
+    normed = (after * factor_of(after) * flat(ffn_gain[...])).astype(BF16)
     for c in range(2):
-        total = toks[c, :, here].astype(F32) + recva[2 * me_z + c].astype(F32)
-        for z in chips:
-            total = total + recva[2 * z + 1 - c].astype(F32)
-        half_after[c] = total
-        eight.append(total)
-    eight = join(eight)
-    tiles = half // lanes
-    gain = jnp.concatenate(
-        [ffn_gain[pl.ds(me_k * tiles + i, 1), :] for i in range(tiles)], axis=1
-    )
-    agf[me_z, :, 0:half] = (eight * gain).astype(BF16)
-    agf[me_z, :, half:] = in_three(jnp.sum(eight * eight, axis=-1, keepdims=True))
-    step = chip_exchange(4, lambda z: agf.at[me_z], agf, me_k)
-    after_copy = pair_copy(3, half_after.at[1 - me_k], after.at[me_k])
-    after[me_k] = half_after[me_k]
+        sendg[c] = normed[:, c * half : (c + 1) * half]
+    step = tp_exchange(4, lambda peer: sendg.at[peer % 2], agf)
+    agf[me_t] = sendg[me_k]
     for i in range(first_ffn, len(loads)):
         loads[i].wait()
     arrive(step)
 
-    unscaled = rows_of(agf, Z).astype(BF16)
-    halves[me_k] = unscaled
-    outgoing = nn(dispatch, unscaled)
+    rows = rows_of(agf, T).astype(BF16)
+    halves[me_k] = rows
+    outgoing = nn(dispatch, rows)
     for j in range(2 * EP):
         sende[j] = outgoing[cap * j : cap * (j + 1)].astype(BF16)
     step = ep_exchange(0, sende, recve)
-    arrive(pair_copy(4, halves.at[me_k], halves.at[me_k]))
-    rows = scaled([halves[c].astype(F32) for c in range(2)])
+    arrive(pair_copy(2, halves.at[me_k], halves.at[me_k]))
+    rows = jnp.concatenate([halves[0], halves[1]], axis=1)
     rows32 = rows.astype(F32)
     act = (silu(nt(rows, v_s[0])) * nt(rows, v_s[1])).astype(BF16)
     ffn = nn(act, v_sd[...])
@@ -470,10 +469,12 @@
 
     for c in range(2):
         ffn_own[c] = ffn[:, c * half : (c + 1) * half]
-    ffn_copy = pair_copy(5, ffn_own.at[1 - me_k], ffn_other)
+    ffn_copy = pair_copy(3, ffn_own.at[1 - me_k], ffn_other)
 
     arrive(step)
-    routed = scaled([join([recve[2 * j + c].astype(F32) for j in range(EP)]) for c in range(2)])
+    routed = jnp.concatenate(
+        [join([recve[2 * j + c].astype(F32) for j in range(EP)]) for c in range(2)], axis=1
+    ).astype(BF16)
     act = (silu(nn(routed, v_e[0])) * nn(routed, v_e[1])).astype(BF16)
     pieces = sendr.shape[0]
     wide = half // pieces
@@ -486,7 +487,6 @@
                 sendr[n, 2 * j + c] = result[cap * j : cap * (j + 1)].astype(BF16)
         steps.append(ep_exchange(1 + n, sendr.at[n], recvr.at[n]))
     arrive(ffn_copy)
-    arrive(after_copy)
     ffn = ffn_own[me_k] + ffn_other[...]
     last = []
     for n in range(pieces):
@@ -501,10 +501,10 @@
     for n in range(pieces):
         arrive(last[n])
         for c in range(2):
-            part = after[c, :, n * wide : (n + 1) * wide]
+            base = c * half + n * wide
+            part = after[:, base : base + wide]
             for z in range(Z):
                 part = part + recvf[n, 2 * z + c].astype(F32)
-            base = c * half + n * wide
             mixed[:, base : base + wide] = part.astype(BF16)
     for c in sends:
         c.wait_send()
@@ -570,7 +570,7 @@
         expert_down[0],
     )
     big = operands[9:]
-    v_in = pltpu.VMEM((2, sum(o.shape[0] for o in big[:3]), width), BF16)
+    v_in = pltpu.VMEM((sum(o.shape[0] for o in big[:3]), width), BF16)
     pair = (2,)
     weights = [v_in] + [
         pltpu.VMEM(shape, BF16)
@@ -578,8 +578,8 @@
         + [pair + o.shape for o in (big[6], big[7], big[8], big[9], big[11])]
         + [big[13].shape, big[14].shape, pair + big[15].shape, big[17].shape]
     ]
-    small = [pltpu.VMEM((2, own, width), BF16)] + [
-        (pltpu.SMEM if o is lengths else pltpu.VMEM)(o.shape, o.dtype) for o in operands[1:9]
+    small = [
+        (pltpu.SMEM if o is lengths else pltpu.VMEM)(o.shape, o.dtype) for o in operands[:9]
     ]
     q_width = latent + lanes
 
@@ -591,15 +591,18 @@
         comm(chips, own, width),
         comm(chips, 2 * R, q_width), comm(chips, 2 * R, q_width),
         comm(chips, 2 * R, latent), comm(chips, 2 * R, latent),
-        comm(T, own, half), comm(T, own, half),
-        pltpu.VMEM((2, own, half), F32), pltpu.VMEM((2, own, half), F32),
-        comm(chips, 2 * own, half + lanes),
-        comm(2, group, half + lanes),
-        comm(2 * EP, cap, half + lanes), comm(2 * EP, cap, half + lanes),
+        comm(chips, own, width), comm(chips, own, width),
+        comm(2, own, half),
+        comm(T, own, half),
+        comm(2, group, half),
+        comm(2 * EP, cap, half), comm(2 * EP, cap, half),
         pltpu.VMEM((2, group, half), F32), pltpu.VMEM((group, half), F32),
         comm(pieces, 2 * EP, cap, half // pieces), comm(pieces, 2 * EP, cap, half // pieces),
         comm(pieces, T, own, half // pieces), comm(pieces, T, own, half // pieces),
         pltpu.VMEM((own, lanes), F32),
+        pltpu.VMEM((q_width // lanes, T * R, lanes), F32),
+        comm(2, width, v_in.shape[0]),
+        comm(own, latent, cache_latent.shape[1]),
     ]
     n_loads = 22
     sems = [
@@ -608,8 +611,8 @@
         pltpu.SemaphoreType.DMA((7,)),
         pltpu.SemaphoreType.DMA((3,)),
         pltpu.SemaphoreType.DMA((3,)),
-        pltpu.SemaphoreType.DMA((8,)),
-        pltpu.SemaphoreType.DMA((8,)),
+        pltpu.SemaphoreType.DMA((6,)),
+        pltpu.SemaphoreType.DMA((6,)),
     ]
     sizes = (T, EP, own, H, nope, rope, latent, cap, (nope + rope) ** (-0.5))
     vmem = pl.BlockSpec(memory_space=pltpu.VMEM)

time: 40.7 us -> 38.9 us (0.956)
  Pallas kernels: 39.8 us -> 38 us
    pallas_call x1, Pallas kernels: 39.2 us -> 37.4 us  [local(): pl.pallas_call(functools.partial(layer, sizes), out_shape=tuple((pltpu.VM...]
where the time goes in v3:
time: 38.9 us; the launch traced here: 38.6 us
  Pallas kernels  38 us (98%)
  between operations  0.65 us (2%)
    pallas_call x1, Pallas kernels, local(): pl.pallas_call(functools.partial(layer, sizes), out_shape=tuple((pltpu.VM...  37.4 us

profile of v3, /device:TPU:0, one launch (start us, length us, event | category | flops | bytes accessed | tf_op | source)
XLA Modules:
  0.0 38.6 jit_solution(1681206159812844117)
XLA Ops:
  0.6 37.4 %shard_map.274 = (bf16[4,2048]{1,0:T(4,128)(2,1)S(1)}, bf16[4,512]{1,0:T(4,128)(2,1)S(1)}, bf16[4,32]{1,0:T(4,128)(2,1)S(1)}) custom-call(bf16[4,2048]{1,0:T(4,128)(2,1)} %h_tokens.1, f32[16,128]{1,0:T(8,128)} %bitcast.40, s32[4]{0:T(128)} %h_lengths.1, f32[22,128]{1,0:T(8,128)} %constant.2.clone.h_turns, s32[4,32]{1,0:T(4,128)} %bitcast.43, ...), custom_call_target="tpu_custom_call" | custom-call | tf_op jit(solution)/shard_map/pallas_call | solution.py:620
  38.0 0.6 %shard_map.275 = (bf16[4,2048]{1,0:T(4,128)(2,1)}, bf16[4,512]{1,0:T(4,128)(2,1)}, bf16[4,32]{1,0:T(4,128)(2,1)}) custom-call(bf16[4,2048]{1,0:T(4,128)(2,1)S(1)} %get-tuple-element.6.refs_0_, bf16[4,512]{1,0:T(4,128)(2,1)S(1)} %get-tuple-element.7.refs_1_, bf16[4,32]{1,0:T(4,128)(2,1)S(1)} %get-tuple-element.8.refs_2_), custom_call_target="tpu_custom_call" | custom-call | tf_op jit(solution)/shard_map/pallas_call | solution.py:628

commit v4 on v3

--- a/solution.py
+++ b/solution.py
@@ -93,7 +93,7 @@
     v_in, v_kr, v_cl, v_cr, v_ku, v_vu, v_wo, v_s, v_d, v_sd, v_dd, v_e, v_ed,
     agx, sendq, recvq, sendo, recvo, senda, recva, sendg, agf, halves,
     sende, recve, ffn_own, ffn_other, sendr, recvr, sendf, recvf,
-    kr_pad, by_row, v_it, v_ct, w_sem, tp_send, tp_recv, ep_send, ep_recv, pair_send, pair_recv,
+    kr_pad, by_row, v_it, v_vt, v_ct, w_sem, tp_send, tp_recv, ep_send, ep_recv, pair_send, pair_recv,
 ):
     T, EP, own, H, nope, rope, latent, cap, scale = sizes
     group = T * own
@@ -217,7 +217,7 @@
     normed = (x * factor_of(x) * flat(attn_gain[...])).astype(BF16)
     agx[me_z] = normed
     loads[2].wait()
-    strip = 2 * lanes
+    strip = 4 * lanes
 
     def turn_weights(i, carry):
         at = pl.ds(pl.multiple_of(i * strip, strip), strip)
@@ -413,10 +413,12 @@
     recvo[me_z] = sendo[me_z]
     for copy in shared:
         arrive(copy)
+    for c in range(2):
+        v_vt[c] = v_vu[c].T
     arrive(step)
 
     back = rows_of(recvo, Z).astype(BF16)
-    value = jnp.concatenate([nt(back, v_vu[c]) for c in range(2)], axis=1)
+    value = jnp.concatenate([nn(back, v_vt[c]) for c in range(2)], axis=1)
     heads = 2 * H
     vhead = value.shape[1] // heads
     at_head = lax.broadcasted_iota(jnp.int32, value.shape, 0) // own % heads
@@ -602,6 +604,7 @@
         pltpu.VMEM((own, lanes), F32),
         pltpu.VMEM((q_width // lanes, T * R, lanes), F32),
         comm(2, width, v_in.shape[0]),
+        comm(2, latent, big[7].shape[0]),
         comm(own, latent, cache_latent.shape[1]),
     ]
     n_loads = 22

time: 38.9 us -> 38.8 us (level)
  no operation moved by 1% of the time
where the time goes in v4:
time: 38.8 us; the launch traced here: 38.6 us
  Pallas kernels  37.9 us (98%)
  between operations  0.65 us (2%)
    pallas_call x1, Pallas kernels, local(): pl.pallas_call(functools.partial(layer, sizes), out_shape=tuple((pltpu.VM...  37.3 us

profile of v4, /device:TPU:0, one launch (start us, length us, event | category | flops | bytes accessed | tf_op | source)
XLA Modules:
  0.0 38.6 jit_solution(12618815946020064404)
XLA Ops:
  0.6 37.3 %shard_map.274 = (bf16[4,2048]{1,0:T(4,128)(2,1)S(1)}, bf16[4,512]{1,0:T(4,128)(2,1)S(1)}, bf16[4,32]{1,0:T(4,128)(2,1)S(1)}) custom-call(bf16[4,2048]{1,0:T(4,128)(2,1)} %h_tokens.1, f32[16,128]{1,0:T(8,128)} %bitcast.40, s32[4]{0:T(128)} %h_lengths.1, f32[22,128]{1,0:T(8,128)} %constant.2.clone.h_turns, s32[4,32]{1,0:T(4,128)} %bitcast.43, ...), custom_call_target="tpu_custom_call" | custom-call | tf_op jit(solution)/shard_map/pallas_call | solution.py:623
  38.0 0.6 %shard_map.275 = (bf16[4,2048]{1,0:T(4,128)(2,1)}, bf16[4,512]{1,0:T(4,128)(2,1)}, bf16[4,32]{1,0:T(4,128)(2,1)}) custom-call(bf16[4,2048]{1,0:T(4,128)(2,1)S(1)} %get-tuple-element.6.refs_0_, bf16[4,512]{1,0:T(4,128)(2,1)S(1)} %get-tuple-element.7.refs_1_, bf16[4,32]{1,0:T(4,128)(2,1)S(1)} %get-tuple-element.8.refs_2_), custom_call_target="tpu_custom_call" | custom-call | tf_op jit(solution)/shard_map/pallas_call | solution.py:631
